TPU v7x, 512 devices: a whole 4x4x16 slice. The times are simulated.
512 devices in a mesh: ep: 32 (over z, core), tp: 16 (over y, x).
Axes of the slice: x: 4, y: 4, z: 16, core: 2. Of those that a mesh axis runs over, the one named last changes fastest.
Arguments:
- query_rows: bfloat16 [24576, 1024], P('ep', 'tp'), may hold values from -600 to 600
- key_rows: bfloat16 [24576, 1024], P('ep', 'tp'), may hold values from -6 to 6
- value_rows: bfloat16 [24576, 1024], P('ep', 'tp'), may hold values from -6 to 6
- cum_gate: float32 [16, 24576], P('tp'), may hold values from -2458 to 0, as said below
- out_weight: bfloat16 [1024, 2048], P(None, 'tp'), may hold values from -0.1875 to 0.1875
- moe_input: bfloat16 [6144, 2048], P('ep'), may hold values from -6 to 6
- moe_gain: float32 [2048], replicated, may hold values from 0.1 to 1.9
- routes: int32 [6144, 3], P('ep'), may hold values from 0 to 127, all different within a row; in each aligned block of 192 rows (0 to 191, 192 to 383, ...) at most 9 rows name the same one
- route_weight: float32 [6144, 3], P('ep'), may hold values from 0.2 to 1.5
- expert_gate: bfloat16 [128, 2048, 512], P('ep', None, 'tp'), may hold values from -0.125 to 0.125
- expert_up: bfloat16 [128, 2048, 512], P('ep', None, 'tp'), may hold values from -0.125 to 0.125
- expert_down: bfloat16 [128, 512, 2048], P('ep', None, 'tp'), may hold values from -0.25 to 0.25
- shared_gate: bfloat16 [2048, 512], P(None, 'tp'), may hold values from -0.125 to 0.125
- shared_up: bfloat16 [2048, 512], P(None, 'tp'), may hold values from -0.125 to 0.125
- shared_down: bfloat16 [512, 2048], P(None, 'tp'), may hold values from -0.25 to 0.25
Outputs:
- mixer_out: bfloat16 [24576, 2048], P('ep', 'tp')
- moe_out: bfloat16 [6144, 2048], P('ep', 'tp')
Inputs may be any that keep to these rules, and one draw needn't show every extreme that they name: Non-increasing along positions: cum_gate[h, t] is the sum of the log forget gates of head h over positions 0 to t. `routes`: the 3 experts of a token differ. In each aligned block of 192 tokens no expert is named by more than 9 tokens, a bound that some block reaches.
All inputs are finite; a program needn't handle non-finite values.
Results may differ from a plain program's by a relative error of at most 0.0068.
Values may be sent and summed in bfloat16 or wider, within the bound.
A program may use at most 64 MiB of HBM per device.

v0:
```python
import functools

import jax
import jax.numpy as jnp
from jax import lax
from jax.experimental import pallas as pl
from jax.experimental.pallas import tpu as pltpu
from jax.sharding import PartitionSpec as P

HEAD = 64
LANES = 128
CORES = 2

neg_fill = -1e30
norm_eps = 1e-06


def attention_kernel(
    heads,
    q_ref,
    kv_ref,
    gate_ref,
    normed_ref,
    rank_ref,
    out_ref,
    tokens,
    picks,
    held,
    acc,
    row_max,
    up_send,
    side_send,
    recv_sem,
    chip_send,
    plane_send,
    piece_recv,
    block_send,
    block_recv,
    own_sem,
    rank_send,
    rank_recv,
):
    rows = kv_ref.shape[0]
    width = kv_ref.shape[1] // 2
    pairs = width // LANES
    tile = 256 if rows % 256 == 0 else rows
    tiles = rows // tile
    me = lax.axis_index("ep")
    chips = lax.axis_size("ep") // CORES
    chip = me // CORES
    core = me % CORES
    other = 1 - core

    barrier = pltpu.get_barrier_semaphore()

    def loop(count, body):
        def step(index, carry):
            body(index)
            return carry

        lax.fori_loop(0, count, step, 0)

    def greet(**where):
        pl.semaphore_signal(barrier, inc=1, device_id=where)

    tp_count = lax.axis_size("tp")
    tp_me = lax.axis_index("tp")
    columns = normed_ref.shape[1] // tp_count

    def chip_at(turn):
        return lax.rem(chip + turn + 1, chips)

    def tp_at(turn):
        return lax.rem(tp_me + turn + 1, tp_count)

    ep_count = chips * CORES

    def ep_at(turn):
        return lax.rem(me + turn + 1, ep_count)

    loop(ep_count - 1, lambda turn: greet(ep=ep_at(turn)))
    loop(tp_count - 1, lambda turn: greet(tp=tp_at(turn)))
    pl.semaphore_wait(barrier, ep_count + tp_count - 2)

    def rank_copy(target, owner):
        return pltpu.make_async_remote_copy(
            src_ref=rank_ref.at[target],
            dst_ref=picks.at[owner],
            send_sem=rank_send.at[target],
            recv_sem=rank_recv.at[owner],
            device_id={"ep": target},
        )

    def up_copy(src, slot):
        return pltpu.make_async_remote_copy(
            src_ref=src,
            dst_ref=held.at[slot],
            send_sem=up_send.at[slot],
            recv_sem=recv_sem.at[slot],
            device_id={"ep": me + CORES},
        )

    def side_copy(src, slot):
        return pltpu.make_async_remote_copy(
            src_ref=src,
            dst_ref=held.at[slot],
            send_sem=side_send.at[slot],
            recv_sem=recv_sem.at[slot],
            device_id={"ep": chip * CORES + other},
        )

    def lanes_of(index):
        return pl.ds(pl.multiple_of(index * columns, columns), columns)

    def chip_copy(target):
        return pltpu.make_async_remote_copy(
            src_ref=normed_ref.at[:, lanes_of(tp_me)],
            dst_ref=tokens.at[me, :, lanes_of(tp_me)],
            send_sem=chip_send.at[target],
            recv_sem=piece_recv.at[me, tp_me],
            device_id={"ep": target * CORES + core},
        )

    def plane_copy(slot, piece, target):
        place = tokens.at[slot, :, lanes_of(piece)]
        return pltpu.make_async_remote_copy(
            src_ref=place,
            dst_ref=place,
            send_sem=plane_send.at[slot, target],
            recv_sem=piece_recv.at[slot, piece],
            device_id={"tp": target},
        )

    def block_copy(src, slot):
        return pltpu.make_async_remote_copy(
            src_ref=src,
            dst_ref=tokens.at[slot],
            send_sem=block_send.at[slot],
            recv_sem=block_recv.at[slot],
            device_id={"ep": chip * CORES + other},
        )

    loop(chips - 1, lambda turn: chip_copy(chip_at(turn)).start())

    @pl.when(chip < chips - 1)
    def _():
        up_copy(kv_ref, me).start()

    @pl.when(core == 0)
    def _():
        side_copy(kv_ref, me).start()

    block_copy(normed_ref, me).start()
    own_copy = pltpu.make_async_copy(normed_ref, tokens.at[me], own_sem)
    own_copy.start()
    loop(ep_count - 1, lambda turn: rank_copy(ep_at(turn), me).start())
    picks[me] = rank_ref[me]

    def spread_pieces(turn):
        slot = chip_at(turn) * CORES + core
        plane_copy(slot, tp_me, tp_me).wait_recv()
        loop(tp_count - 1, lambda way: plane_copy(slot, tp_me, tp_at(way)).start())

    def share_blocks(turn):
        slot = chip_at(turn) * CORES + core
        loop(tp_count - 1, lambda way: plane_copy(slot, tp_at(way), tp_me).wait_recv())
        block_copy(tokens.at[slot], slot).start()

    ones = jnp.ones((rows, LANES), jnp.bfloat16)

    def block_step(block, source, first):
        for pair in range(pairs):
            lanes = pl.ds(pair * LANES, LANES)
            value_lanes = pl.ds(width + pair * LANES, LANES)

            def one_tile(index, carry):
                start = pl.multiple_of(index * tile, tile)
                q_rows = pl.ds(start, tile)
                gates = gate_ref[pl.ds(pl.multiple_of(block * rows, rows), rows), lanes]
                keys = jnp.concatenate([source[:, lanes], gates], axis=1)
                values = jnp.concatenate([source[:, value_lanes], ones], axis=1)
                for head in range(2 * pair, min(2 * pair + 2, heads)):
                    scores = lax.dot_general(
                        q_ref[head, q_rows, :],
                        keys,
                        (((1,), (1,)), ((), ())),
                        preferred_element_type=jnp.float32,
                    )
                    if first:
                        q_pos = start + lax.broadcasted_iota(jnp.int32, scores.shape, 0)
                        k_pos = lax.broadcasted_iota(jnp.int32, scores.shape, 1)
                        scores = jnp.where(k_pos <= q_pos, scores, neg_fill)
                        top = jnp.max(scores, axis=1, keepdims=True)
                        new_max = jnp.broadcast_to(top, (tile, LANES))
                    else:
                        old_max = row_max[head, q_rows, :]
                        new_max = jnp.maximum(old_max, jnp.max(scores, axis=1, keepdims=True))
                    probs = jnp.exp(scores - new_max[:, :1]).astype(jnp.bfloat16)
                    add = jnp.dot(probs, values, preferred_element_type=jnp.float32)
                    if not first:
                        keep = jnp.exp(old_max - new_max)
                        add = add + acc[head, q_rows, :] * jnp.concatenate([keep, keep], axis=1)
                    acc[head, q_rows, :] = add
                    row_max[head, q_rows, :] = new_max
                return carry

            lax.fori_loop(0, tiles, one_tile, 0)

    block_step(me, kv_ref, True)
    loop(chips - 1, spread_pieces)

    @pl.when(me == 0)
    def _():
        loop(chips - 1, share_blocks)

    def remote_step(step, carry):
        turn = step - core + 2
        own_core = turn % 2 == 0
        slot = (chip - turn // 2) * CORES + jnp.where(own_core, core, other)
        landed = held.at[slot]
        side_copy(landed, slot).wait_recv()

        @pl.when(jnp.logical_and(own_core, chip < chips - 1))
        def _():
            up_copy(landed, slot).start()

        @pl.when(own_core)
        def _():
            side_copy(landed, slot).start()

        @pl.when(step == jnp.maximum(me - 2, 0))
        def _():
            loop(chips - 1, share_blocks)

        block_step(slot, landed, False)
        return carry

    lax.fori_loop(0, me, remote_step, 0)

    for head in range(heads):
        pair, part = head // 2, head % 2
        spot = slice(part * HEAD, part * HEAD + HEAD)
        whole = acc[head, :, :LANES] / acc[head, :, LANES:]
        out_ref[:, head * HEAD : (head + 1) * HEAD] = whole[:, spot].astype(out_ref.dtype)

    def finish(step):
        slot = (chip - step) * CORES + core

        @pl.when(chip < chips - 1)
        def _():
            up_copy(held.at[slot], slot).wait_send()

        @pl.when(step > 0)
        def _():
            side_copy(held.at[slot], slot).wait_send()

    loop(chip + 1, finish)

    @pl.when(core == 0)
    def _():
        side_copy(kv_ref, me).wait_send()

    def finish_tokens(turn):
        target = chip_at(turn)
        slot = target * CORES + core
        chip_copy(target).wait_send()
        loop(tp_count - 1, lambda way: plane_copy(slot, tp_me, tp_at(way)).wait_send())
        block_copy(tokens.at[slot], slot).wait_send()

    loop(chips - 1, finish_tokens)
    block_copy(normed_ref, me).wait_send()

    def finish_blocks(index):
        slot = index * CORES + other
        block_copy(tokens.at[slot], slot).wait_recv()

    loop(chips, finish_blocks)
    own_copy.wait()

    def finish_ranks(turn):
        rank_copy(ep_at(turn), me).wait_send()
        rank_copy(ep_at(turn), ep_at(turn)).wait_recv()

    loop(ep_count - 1, finish_ranks)


def exchange_kernel(count, *refs):
    sources, targets = refs[:count], refs[count : 2 * count]
    send_sem, recv_sem, own_sem = refs[2 * count :]
    tp_count = lax.axis_size("tp")
    tp_me = lax.axis_index("tp")
    barrier = pltpu.get_barrier_semaphore()
    ways = [lax.rem(tp_me + turn, tp_count) for turn in range(1, tp_count)]
    for way in ways:
        pl.semaphore_signal(barrier, inc=1, device_id={"tp": way})
    pl.semaphore_wait(barrier, tp_count - 1)

    def place(index, owner):
        span = sources[index].shape[1]
        if span % LANES:
            return targets[index].at[owner]
        return targets[index].at[:, pl.ds(pl.multiple_of(owner * span, span), span)]

    def copy(index, way, owner):
        return pltpu.make_async_remote_copy(
            src_ref=sources[index],
            dst_ref=place(index, owner),
            send_sem=send_sem.at[index, way],
            recv_sem=recv_sem.at[index, owner],
            device_id={"tp": way},
        )

    for index in range(count):
        for way in ways:
            copy(index, way, tp_me).start()
    own = [
        pltpu.make_async_copy(sources[index], place(index, tp_me), own_sem.at[index])
        for index in range(count)
    ]
    for one in own:
        one.start()
    for one in own:
        one.wait()
    for index in range(count):
        for way in ways:
            copy(index, way, way).wait_recv()
            copy(index, way, tp_me).wait_send()


def exchange(collective_id, *arrays):
    tp_count = lax.axis_size("tp")
    count = len(arrays)

    def gathered(a):
        rows, span = a.shape
        shape = (tp_count, rows, span) if span % LANES else (rows, tp_count * span)
        return jax.ShapeDtypeStruct(shape, a.dtype)

    results = pl.pallas_call(
        functools.partial(exchange_kernel, count),
        out_shape=[gathered(a) for a in arrays],
        in_specs=[pl.BlockSpec(memory_space=pltpu.VMEM)] * count,
        out_specs=[pl.BlockSpec(memory_space=pltpu.VMEM)] * count,
        scratch_shapes=[
            pltpu.SemaphoreType.DMA((count, tp_count)),
            pltpu.SemaphoreType.DMA((count, tp_count)),
            pltpu.SemaphoreType.DMA((count,)),
        ],
        compiler_params=pltpu.CompilerParams(collective_id=collective_id, has_side_effects=True),
        cost_estimate=pl.CostEstimate(flops=0, bytes_accessed=24 * 1024 * 1024, transcendentals=0),
        name="exchange",
    )(*arrays)
    return [
        r if r.ndim == 2 else r.transpose(1, 0, 2).reshape(r.shape[1], -1) for r in results
    ]


def attention(query_rows, key_rows, value_rows, cum_gate, normed, ranks):
    rows, width = query_rows.shape
    heads = width // HEAD
    pairs = (heads + 1) // 2
    ep_count = lax.axis_size("ep")
    padded = pairs * LANES
    if padded > width:
        spare = ((0, 0), (0, padded - width))
        query_rows, key_rows, value_rows = (
            jnp.pad(a, spare) for a in (query_rows, key_rows, value_rows)
        )
    key_value = jnp.concatenate([key_rows, value_rows], axis=1)
    scaled = query_rows * jnp.asarray(HEAD**-0.5, jnp.bfloat16)
    lane = jnp.arange(LANES)
    parts = []
    for head in range(heads):
        pair, part = head // 2, head % 2
        piece = scaled[:, pair * LANES : (pair + 1) * LANES]
        piece = jnp.where((lane // HEAD == part)[None], piece, 0)
        marks = ((lane // 3) == part).astype(jnp.bfloat16)
        parts.append(jnp.concatenate([piece, jnp.broadcast_to(marks, (rows, LANES))], axis=1))
    queries = jnp.stack(parts)
    minus = -cum_gate
    high = lax.reduce_precision(minus, 8, 7)
    rest = minus - high
    mid = lax.reduce_precision(rest, 8, 7)
    low = rest - mid
    terms = jnp.concatenate([high, mid, low], axis=0).astype(jnp.bfloat16)
    source = jnp.arange(3 * heads)
    spot = (source % heads // 2) * LANES + (source % heads % 2) * 3 + source // heads
    layout = (spot[:, None] == jnp.arange(padded)[None, :]).astype(jnp.bfloat16)
    gates = lax.dot_general(
        terms, layout, (((0,), (0,)), ((), ())), preferred_element_type=jnp.float32
    ).astype(jnp.bfloat16)
    blocks = ep_count * rows * rows * heads
    return pl.pallas_call(
        functools.partial(attention_kernel, heads),
        out_shape=[
            jax.ShapeDtypeStruct((rows, heads * HEAD), jnp.bfloat16),
            jax.ShapeDtypeStruct((ep_count,) + normed.shape, jnp.bfloat16),
            jax.ShapeDtypeStruct(ranks.shape, jnp.bfloat16),
        ],
        in_specs=[pl.BlockSpec(memory_space=pltpu.VMEM)] * 5,
        out_specs=[
            pl.BlockSpec(memory_space=pltpu.VMEM),
            pl.BlockSpec(memory_space=pl.ANY),
            pl.BlockSpec(memory_space=pltpu.VMEM),
        ],
        scratch_shapes=[
            pltpu.VMEM((ep_count, rows, 2 * padded), jnp.bfloat16),
            pltpu.VMEM((heads, rows, 2 * LANES), jnp.float32),
            pltpu.VMEM((heads, rows, LANES), jnp.float32),
            pltpu.SemaphoreType.DMA((ep_count,)),
            pltpu.SemaphoreType.DMA((ep_count,)),
            pltpu.SemaphoreType.DMA((ep_count,)),
            pltpu.SemaphoreType.DMA((ep_count,)),
            pltpu.SemaphoreType.DMA((ep_count, lax.axis_size("tp"))),
            pltpu.SemaphoreType.DMA((ep_count, lax.axis_size("tp"))),
            pltpu.SemaphoreType.DMA((ep_count,)),
            pltpu.SemaphoreType.DMA((ep_count,)),
            pltpu.SemaphoreType.DMA,
            pltpu.SemaphoreType.DMA((ep_count,)),
            pltpu.SemaphoreType.DMA((ep_count,)),
        ],
        compiler_params=pltpu.CompilerParams(
            collective_id=0, has_side_effects=True, vmem_limit_bytes=48 * 1024 * 1024
        ),
        cost_estimate=pl.CostEstimate(
            flops=blocks * 2 * 512, bytes_accessed=8 * 1024 * 1024, transcendentals=blocks
        ),
        name="attend",
    )(queries, key_value, gates, normed, ranks)


def local(
    query_rows,
    key_rows,
    value_rows,
    cum_gate,
    out_weight,
    moe_input,
    moe_gain,
    routes,
    route_weight,
    expert_gate,
    expert_up,
    expert_down,
    shared_gate,
    shared_up,
    shared_down,
):
    token_count = moe_input.shape[0]
    top_count = routes.shape[1]
    local_experts = expert_gate.shape[0]
    ep_count = lax.axis_size("ep")
    expert_count = local_experts * ep_count
    capacity = 2 * token_count * top_count // expert_count
    column_count = expert_down.shape[2]
    first_column = lax.axis_index("tp") * column_count
    moe_rows = moe_input.astype(jnp.float32)
    normed = (
        moe_rows
        * lax.rsqrt(jnp.mean(moe_rows * moe_rows, axis=1, keepdims=True) + norm_eps)
        * moe_gain
    ).astype(jnp.bfloat16)
    expert_ids = jnp.arange(expert_count, dtype=jnp.int32)
    chosen = routes[:, :, None] == expert_ids[None, None, :]
    named = jnp.any(chosen, axis=1)
    weight_of = jnp.sum(jnp.where(chosen, route_weight[:, :, None], 0.0), axis=1)
    order = jnp.arange(token_count)
    earlier = (order[None, :] < order[:, None]).astype(jnp.bfloat16)
    ranks = jnp.dot(earlier, named.astype(jnp.bfloat16), preferred_element_type=jnp.float32)
    ranks = jnp.where(named, ranks.astype(jnp.int32), -1)
    slots = jnp.arange(capacity, dtype=jnp.int32)
    place = ranks[:, :, None] == slots[None, None, :]
    rank_rows = ranks.astype(jnp.bfloat16).T.reshape(ep_count, local_experts, token_count)
    heads_out, tokens, mine = attention(
        query_rows, key_rows, value_rows, cum_gate, normed, rank_rows
    )
    pick = mine[:, :, None, :] == slots.astype(jnp.bfloat16)[None, None, :, None]
    pick = pick.astype(jnp.bfloat16).reshape(ep_count, local_experts * capacity, token_count)
    arrived = jnp.einsum("ast,atd->asd", pick, tokens, preferred_element_type=jnp.float32)
    arrived = arrived.astype(jnp.bfloat16).reshape(ep_count, local_experts, capacity, -1)
    gate_val = jnp.einsum(
        "aecd,edf->aecf", arrived, expert_gate, preferred_element_type=jnp.float32
    )
    up_val = jnp.einsum("aecd,edf->aecf", arrived, expert_up, preferred_element_type=jnp.float32)
    hidden = (jax.nn.silu(gate_val) * up_val).astype(jnp.bfloat16)
    shared_hidden = (
        jax.nn.silu(jnp.dot(normed, shared_gate, preferred_element_type=jnp.float32))
        * jnp.dot(normed, shared_up, preferred_element_type=jnp.float32)
    ).astype(jnp.bfloat16)
    slot_count = ep_count * local_experts * capacity
    by_expert = hidden.transpose(1, 0, 2, 3).reshape(slot_count, hidden.shape[3])
    hidden, shared_all = exchange(1, by_expert, shared_hidden)
    hidden = hidden.reshape(local_experts, ep_count * capacity, -1)
    result = jnp.einsum("esf,efd->esd", hidden, expert_down, preferred_element_type=jnp.float32)
    result = result.astype(jnp.bfloat16).reshape(local_experts, ep_count, capacity, column_count)
    result = result.transpose(1, 0, 2, 3)
    result, heads_out = lax.optimization_barrier((result, heads_out))
    returned = lax.all_to_all(result, "ep", split_axis=0, concat_axis=0, tiled=True)
    returned = returned.reshape(expert_count * capacity, column_count)
    weight_high = lax.reduce_precision(weight_of, 8, 7)
    weight_low = weight_of - weight_high
    routed = 0.0
    for weight in (weight_high, weight_low):
        spread = jnp.where(place, weight[:, :, None], 0.0).astype(jnp.bfloat16)
        routed = routed + jnp.dot(
            spread.reshape(token_count, expert_count * capacity),
            returned,
            preferred_element_type=jnp.float32,
        )
    (heads_all,) = exchange(2, heads_out)
    mixer_sum = jnp.dot(heads_all, out_weight, preferred_element_type=jnp.float32)
    moe_total = routed + jnp.dot(shared_all, shared_down, preferred_element_type=jnp.float32)
    return (mixer_sum.astype(jnp.bfloat16), moe_total.astype(jnp.bfloat16))


def solution(mesh):
    placed = (
        P("ep", "tp"),
        P("ep", "tp"),
        P("ep", "tp"),
        P("tp", None),
        P(None, "tp"),
        P("ep", None),
        P(),
        P("ep", None),
        P("ep", None),
        P("ep", None, "tp"),
        P("ep", None, "tp"),
        P("ep", None, "tp"),
        P(None, "tp"),
        P(None, "tp"),
        P(None, "tp"),
    )
    return jax.shard_map(
        local, mesh=mesh, in_specs=placed, out_specs=(P("ep", "tp"), P("ep", "tp")), check_vma=False
    )
```

profile of v0, /device:TPU:1, one launch (start us, length us, event | category | flops | bytes accessed | tf_op | source)
XLA Modules:
  0.0 432.7 jit_solution(10424242617294190451)
XLA Ops:
  0.6 0.0 copy-start
  0.7 1.2 reduce-precision_convert_fusion.1
  1.9 1.4 fusion
  3.3 0.8 fusion.20
  4.2 0.2 fusion.11
  4.4 0.1 copy.72
  4.5 1.1 copy.69
  5.6 0.2 copy.70
  5.8 0.2 copy.71
  5.9 0.3 fusion.2.normed_ref
  6.2 0.1 multiply_select_fusion
  6.3 0.1 maximum_bitcast_fusion.q_ref
  6.4 0.1 fusion.19.kv_ref
  6.4 4.4 %convolution_convert_fusion.gate_ref = bf16[24576,128]{1,0:T(8,128)(2,1)} fusion(bf16[1,24576]{1,0:T(2,128)(2,1)S(1)} %get-tuple-element.21, bf16[1,24576]{1,0:T(2,128)(2,1)S(1)} %get-tuple-element.22, bf16[1,24576]{1,0:T(2,128)(2,1)S(1)} %get-tuple-element.20), kind=kOutput, calls=%fused_computation | convolution fusion | flops 22462848 | bytes 6438912 | tf_op jit(solution)/shard_map/dot_general | solution.py:389
  10.9 199.6 %attend.1 = (bf16[768,64]{1,0:T(8,128)(2,1)S(1)}, bf16[32,192,2048]{2,1,0:T(8,128)(2,1)}, bf16[32,4,192]{2,1,0:T(4,128)(2,1)S(1)}) custom-call(bf16[1,768,256]{2,1,0:T(8,128)(2,1)S(1)} %maximum_bitcast_fusion.q_ref, bf16[768,256]{1,0:T(8,128)(2,1)S(1)} %fusion.19.kv_ref, bf16[24576,128]{1,0:T(8,128)(2,1)} %convolution_convert_fusion.gate_ref, ...), custom_call_target="tpu_custom_call" | custom-call | flops 19327352832 | bytes 8388608 | tf_op jit(solution)/shard_map/attend/pallas_call | solution.py:393
  210.5 0.7 copy-done.1
  211.2 0.1 eq.100
  211.3 0.2 bitcast_compare_fusion
  211.5 15.0 %convolution_convert_fusion.1 = bf16[32,36,2048]{2,1,0:T(8,128)(2,1)} fusion(bf16[32,192,2048]{2,1,0:T(8,128)(2,1)} %get-tuple-element.10, pred[32,36,192]{2,0,1:T(32,128)(4,1)S(1)} %bitcast_compare_fusion), kind=kOutput, calls=%fused_computation.1 | convolution fusion | flops 908328960 | bytes 30105600 | tf_op jit(solution)/shard_map/ast,atd->asd/dot_general | solution.py:479
  226.5 5.1 %copy.75 = bf16[32,36,2048]{2,0,1:T(8,128)(2,1)S(1)} copy(bf16[32,36,2048]{2,1,0:T(8,128)(2,1)} %convolution_convert_fusion.1) | data formatting | bytes 9437184 | tf_op jit(solution)/shard_map/convert_element_type | solution.py:480
  231.7 1.4 fusion.17
  233.1 1.4 fusion.6
  234.5 0.2 copy.76
  234.6 1.1 reshape.142.refs_0_
  235.8 0.3 fusion.29
  236.1 1.0 fusion.12.refs_1_
  237.1 100.0 %exchange.2 = (bf16[16,1152,32]{2,1,0:T(8,128)(2,1)}, bf16[16,192,32]{2,1,0:T(8,128)(2,1)}) custom-call(bf16[1152,32]{1,0:T(8,128)(2,1)} %reshape.142.refs_0_, bf16[192,32]{1,0:T(8,128)(2,1)} %fusion.12.refs_1_), custom_call_target="tpu_custom_call" | custom-call | bytes 25165824 | tf_op jit(solution)/shard_map/exchange/pallas_call | solution.py:339
  337.1 3.8 copy.82
  340.9 1.4 reshape_reshape.3
  342.4 0.6 fusion.7
  343.0 0.9 copy.84
  343.9 20.0 %all-to-all-start = ((bf16[32,4,9,128]{3,1,2,0:T(4,128)(2,1)}), bf16[32,4,9,128]{3,1,2,0:T(4,128)(2,1)}, u32[]{:S(2)}, u32[]{:S(2)}) async-start(bf16[32,4,9,128]{3,1,2,0:T(4,128)(2,1)} %bitcast.10), calls=%async_computation | async-start | bytes 589824 | tf_op jit(solution)/shard_map/all_to_all | solution.py:498
  363.9 0.1 copy.86
  364.0 0.2 select_reduce_fusion
  364.2 0.1 copy.87
  364.4 0.1 copy.89
  364.5 0.8 select_convert_fusion
  365.3 0.4 convert_element_type.101
  365.7 1.4 copy.90
  367.2 0.4 convert_element_type.103
  367.6 55.3 %exchange.3 = bf16[16,768,64]{2,1,0:T(8,128)(2,1)} custom-call(bf16[768,64]{1,0:T(8,128)(2,1)} %copy-done.1), custom_call_target="tpu_custom_call" | custom-call | bytes 25165824 | tf_op jit(solution)/shard_map/exchange/pallas_call | solution.py:339
  422.9 3.1 copy.85
  426.0 1.8 fusion.31
  427.8 2.3 convolution_convert_fusion.2
  430.1 1.1 copy.88
  431.2 0.1 reshape.145
  431.3 0.4 fusion.30
  431.7 1.0 fusion.13
  (35 shorter events, 0.2 us)
Async XLA Ops:
  0.6 341.7 %copy-start = (bf16[4,512,128]{2,1,0:T(8,128)(2,1)S(1)}, bf16[4,512,128]{2,1,0:T(8,128)(2,1)}, u32[]{:S(2)}) copy-start(bf16[4,512,128]{2,1,0:T(8,128)(2,1)} %param.26) | copy-start | bytes 1572868
  0.6 5.3 %copy-start.2 = (bf16[192,2048]{1,0:T(8,128)(2,1)S(1)}, bf16[192,2048]{1,0:T(8,128)(2,1)}, u32[]{:S(2)}) copy-start(bf16[192,2048]{1,0:T(8,128)(2,1)} %param.20) | copy-start | bytes 2359300
  0.7 4.9 %copy-start.5 = (bf16[768,64]{0,1:T(8,128)(2,1)S(1)}, bf16[768,64]{0,1:T(8,128)(2,1)}, u32[]{:S(2)}) copy-start(bf16[768,64]{0,1:T(8,128)(2,1)} %param.16) | copy-start | bytes 294916
  0.7 5.1 %copy-start.6 = (bf16[768,64]{0,1:T(8,128)(2,1)S(1)}, bf16[768,64]{0,1:T(8,128)(2,1)}, u32[]{:S(2)}) copy-start(bf16[768,64]{0,1:T(8,128)(2,1)} %param.17) | copy-start | bytes 294916
  0.7 5.3 %copy-start.8 = (f32[2048]{0:T(1024)S(1)}, f32[2048]{0:T(1024)}, u32[]{:S(2)}) copy-start(f32[2048]{0:T(1024)} %param.21) | copy-start | bytes 24580
  210.5 0.7 copy-start.1
  226.5 5.1 %copy-start.10 = (bf16[4,2048,32]{1,2,0:T(8,128)(2,1)S(1)}, bf16[4,2048,32]{1,2,0:T(8,128)(2,1)}, u32[]{:S(2)}) copy-start(bf16[4,2048,32]{1,2,0:T(8,128)(2,1)} %param.24) | copy-start | bytes 1572868
  231.7 1.4 copy-start.11
  233.1 2.7 copy-start.4
  234.5 1.6 copy-start.12
  342.4 21.6 %copy-start.7 = (s32[192,3]{0,1:T(4,128)S(1)}, s32[192,3]{0,1:T(4,128)}, u32[]{:S(2)}) copy-start(s32[192,3]{0,1:T(4,128)} %param.22) | copy-start | bytes 6916
  342.4 21.6 %copy-start.9 = (f32[192,3]{0,1:T(4,128)S(1)}, f32[192,3]{0,1:T(4,128)}, u32[]{:S(2)}) copy-start(f32[192,3]{0,1:T(4,128)} %param.23) | copy-start | bytes 6916
  343.9 86.2 %all-to-all-start = ((bf16[32,4,9,128]{3,1,2,0:T(4,128)(2,1)}), bf16[32,4,9,128]{3,1,2,0:T(4,128)(2,1)}, u32[]{:S(2)}, u32[]{:S(2)}) async-start(bf16[32,4,9,128]{3,1,2,0:T(4,128)(2,1)} %bitcast.10), calls=%async_computation | async-start | bytes 589824 | tf_op jit(solution)/shard_map/all_to_all | solution.py:498
  427.8 3.9 copy-start.3
where the time goes:
time: 433 us
  Pallas kernels  355 us (82%)
  matrix products  29.7 us (7%)
  local copies, waits for them, and re-layouts  21.8 us (5%)
  starting transfers between devices  20 us (5%)
  other arithmetic  5.16 us (1%)
    pallas_call x1, Pallas kernels, attention(): pl.pallas_call(functools.partial(attention_kernel, heads), out_shape=[jax...  200 us
    pallas_call x2, Pallas kernels, exchange(): pl.pallas_call(functools.partial(exchange_kernel, count), out_shape=[gath...  155 us
    all_to_all x1, starting transfers between devices, local(): lax.all_to_all(result, 'ep', split_axis=0, concat_axis=0, tiled=True)  20 us
    dot_general x1, matrix products, local(): jnp.einsum('ast,atd->asd', pick, tokens, preferred_element_type=jnp.float32)  15 us
  transfers between devices with their start and end apart: 1, of which 0 were waited for; matrix products, arithmetic and copies ran while one was open for 3% of the time, Pallas kernels for 13%

commit v1 on v0

v1 whole, which is shorter than its diff:
```python
import functools

import jax
import jax.numpy as jnp
import numpy as np
from jax import lax
from jax.experimental import pallas as pl
from jax.experimental.pallas import tpu as pltpu
from jax.sharding import PartitionSpec as P

HEAD = 64
LANES = 128
CORES = 2
TERMS = 4
LOG2E = 1.4426950408889634

neg_fill = -1e30
norm_eps = 1e-06

GATHER_AT = 10
PARTS_AT = 16
HIDDEN_AT = 20
DOWN_AT = 26


def plane_shape(tp_count):
    wide = 1
    while wide * wide < tp_count:
        wide *= 2
    return wide, tp_count // wide


def dot(a, b):
    return jnp.dot(a, b, preferred_element_type=jnp.float32)


def dot_nt(a, b):
    return lax.dot_general(a, b, (((1,), (1,)), ((), ())), preferred_element_type=jnp.float32)


def silu(v):
    return v / (1.0 + jnp.exp(-v))


def loop(count, body, first=0):
    def step(index, carry):
        body(index)
        return carry

    lax.fori_loop(first, count, step, 0)


def layer_kernel(
    cap,
    room,
    q_ref,
    kv_ref,
    terms_ref,
    normed_ref,
    ranks_ref,
    weight_ref,
    places_ref,
    owner_ref,
    gate_w,
    up_w,
    down_ref,
    shared_gate_ref,
    shared_up_ref,
    shared_down_ref,
    out_weight_ref,
    mixer_ref,
    moe_ref,
    held,
    acc,
    row_max,
    picked,
    pieces,
    weights,
    part_out,
    part_in,
    hidden_out,
    hidden_all,
    result_out,
    result_in,
    spread,
    heads_out,
    heads_all,
    up_send,
    down_send,
    side_send,
    kv_recv,
    pick_send,
    pick_recv,
    result_send,
    result_recv,
    piece_send,
    piece_recv,
    weight_send,
    weight_recv,
    part_send,
    part_recv,
    hidden_send,
    hidden_recv,
    head_send,
    head_recv,
    own_sem,
):
    rows = q_ref.shape[1]
    half = rows // 2
    chunks = rows // LANES
    tile = 256 if rows % 256 == 0 else rows
    tokens = normed_ref.shape[0]
    experts = gate_w.shape[0]
    own_hidden = gate_w.shape[1]
    slot_count = picked.shape[0]
    slot_tile = 256 if slot_count % 256 == 0 else slot_count
    slot_span = -(-slot_count // LANES) * LANES

    me = lax.axis_index("ep")
    ep_count = lax.axis_size("ep")
    chips = ep_count // CORES
    chip = me // CORES
    core = me % CORES
    other = 1 - core
    tp_count = lax.axis_size("tp")
    tp_me = lax.axis_index("tp")
    wide, tall = plane_shape(tp_count)
    x_me = tp_me % wide
    y_me = tp_me // wide
    up_hops = chips // 2
    down_hops = chips - 1 - up_hops
    last_down = chips - 2 - up_hops
    features = normed_ref.shape[1] // wide

    def ep_at(turn):
        return lax.rem(me + turn + 1, ep_count)

    def tp_at(turn):
        return lax.rem(tp_me + turn + 1, tp_count)

    def x_at(turn):
        return lax.rem(x_me + turn + 1, wide)

    def y_at(turn):
        return lax.rem(y_me + turn + 1, tall)

    barrier = pltpu.get_barrier_semaphore()

    def greet(**where):
        pl.semaphore_signal(barrier, inc=1, device_id=where)

    loop(ep_count - 1, lambda turn: greet(ep=ep_at(turn)))
    loop(tp_count - 1, lambda turn: greet(tp=tp_at(turn)))

    def room_of(index):
        return pl.ds(pl.multiple_of(index * room, 8), room)

    def feature_lanes(index):
        return pl.ds(pl.multiple_of(index * features, LANES), features)

    piece_lanes = pl.ds(pl.multiple_of(x_me * features + y_me * LANES, LANES), LANES)
    column = lax.broadcasted_iota(jnp.int32, (tokens, LANES), 1)
    marker = jnp.where(column == 0, 1.0, 0.0).astype(jnp.bfloat16)
    ranks = jnp.concatenate([ranks_ref[...], marker], axis=1)
    own_piece = normed_ref[:, piece_lanes]
    for start in range(0, slot_count, slot_tile):
        span = slice(start, start + slot_tile)
        match = dot_nt(places_ref[span, :], ranks)
        pick = jnp.where(match == 0.0, 1.0, 0.0).astype(jnp.bfloat16)
        rows_of = dot(pick, own_piece).astype(jnp.bfloat16)
        picked[span, :] = rows_of

    acc[...] = jnp.zeros_like(acc)
    row_max[...] = jnp.full_like(row_max, neg_fill)

    pl.semaphore_wait(barrier, ep_count + tp_count - 2)

    def pick_copy(target, owner):
        return pltpu.make_async_remote_copy(
            src_ref=picked.at[room_of(target)],
            dst_ref=pieces.at[y_me, room_of(owner)],
            send_sem=pick_send.at[target],
            recv_sem=pick_recv.at[owner],
            device_id={"ep": target},
        )

    def weight_copy(source, index, target, owner):
        return pltpu.make_async_remote_copy(
            src_ref=source.at[:, :, feature_lanes(target)],
            dst_ref=weights.at[owner, index],
            send_sem=weight_send.at[index, target],
            recv_sem=weight_recv.at[index, owner],
            device_id={"tp": y_me * wide + target},
        )

    def own_weight(source, index):
        return pltpu.make_async_copy(
            source.at[:, :, feature_lanes(x_me)], weights.at[x_me, index], own_sem.at[index]
        )

    def up_copy(src, slot):
        return pltpu.make_async_remote_copy(
            src_ref=src,
            dst_ref=held.at[slot],
            send_sem=up_send.at[slot],
            recv_sem=kv_recv.at[slot],
            device_id={"ep": me + CORES},
        )

    def down_copy(src, slot):
        return pltpu.make_async_remote_copy(
            src_ref=src,
            dst_ref=held.at[slot],
            send_sem=down_send.at[slot],
            recv_sem=kv_recv.at[slot],
            device_id={"ep": lax.rem(chip + chips - 1, chips) * CORES + core},
        )

    def side_copy(src, slot):
        return pltpu.make_async_remote_copy(
            src_ref=src,
            dst_ref=held.at[slot],
            send_sem=side_send.at[slot],
            recv_sem=kv_recv.at[slot],
            device_id={"ep": chip * CORES + other},
        )

    def piece_copy(target, owner):
        return pltpu.make_async_remote_copy(
            src_ref=pieces.at[owner],
            dst_ref=pieces.at[owner],
            send_sem=piece_send.at[target],
            recv_sem=piece_recv.at[owner],
            device_id={"tp": target * wide + x_me},
        )

    def part_copy(target, owner):
        return pltpu.make_async_remote_copy(
            src_ref=part_out.at[target],
            dst_ref=part_in.at[owner],
            send_sem=part_send.at[target],
            recv_sem=part_recv.at[owner],
            device_id={"tp": y_me * wide + target},
        )

    def hidden_copy(target, owner):
        return pltpu.make_async_remote_copy(
            src_ref=hidden_out,
            dst_ref=hidden_all.at[owner],
            send_sem=hidden_send.at[target],
            recv_sem=hidden_recv.at[owner],
            device_id={"tp": target},
        )

    def result_copy(target, owner):
        return pltpu.make_async_remote_copy(
            src_ref=result_out.at[room_of(target)],
            dst_ref=result_in.at[room_of(owner)],
            send_sem=result_send.at[target],
            recv_sem=result_recv.at[owner],
            device_id={"ep": target},
        )

    def own_result():
        return pltpu.make_async_copy(
            result_out.at[room_of(me)], result_in.at[room_of(me)], own_sem.at[2]
        )

    def head_copy(target, owner):
        return pltpu.make_async_remote_copy(
            src_ref=heads_out,
            dst_ref=heads_all.at[owner],
            send_sem=head_send.at[target],
            recv_sem=head_recv.at[owner],
            device_id={"tp": target},
        )

    def own_pick():
        return pltpu.make_async_copy(
            picked.at[room_of(me)], pieces.at[y_me, room_of(me)], own_sem.at[3]
        )

    loop(ep_count - 1, lambda turn: pick_copy(ep_at(turn), me).start())
    own_pick().start()

    @pl.when(chip < chips - 1)
    def _():
        up_copy(kv_ref, me).start()

    @pl.when(chip <= last_down)
    def _():
        down_copy(kv_ref, me).start()

    @pl.when(core == 0)
    def _():
        side_copy(kv_ref, me).start()

    def start_weights(turn):
        weight_copy(gate_w, 0, x_at(turn), x_me).start()
        weight_copy(up_w, 1, x_at(turn), x_me).start()

    loop(wide - 1, start_weights)
    own_weight(gate_w, 0).start()
    own_weight(up_w, 1).start()

    ones = jnp.ones((acc.shape[0] - HEAD, rows), jnp.bfloat16)
    nothing = jnp.zeros((HEAD, tile), jnp.bfloat16)

    def block_step(block, source, masked):
        mark = lax.broadcasted_iota(jnp.int32, (LANES, tile), 0)
        wanted = jnp.logical_and(mark // TERMS == block, mark % TERMS < TERMS - 1)
        chosen = jnp.where(wanted, 1.0, 0.0).astype(jnp.bfloat16)
        keys = source[0:half, :]
        early = jnp.concatenate([keys, terms_ref[0:half, :]], axis=1)
        late = jnp.concatenate([keys, terms_ref[half:rows, :]], axis=1)
        values = jnp.concatenate(
            [source[half + HEAD * i : half + HEAD * (i + 1), :] for i in range(chunks)], axis=1
        )
        values = jnp.concatenate([values, ones], axis=0)
        for start in range(0, rows, tile):
            span = slice(start, start + tile)
            query = q_ref[:, span]
            first = dot(early, jnp.concatenate([query, nothing, chosen], axis=0))
            second = dot(late, jnp.concatenate([nothing, query, chosen], axis=0))
            if masked:
                q_pos = start + lax.broadcasted_iota(jnp.int32, first.shape, 1)
                k_pos = lax.broadcasted_iota(jnp.int32, first.shape, 0)
                first = jnp.where(k_pos <= q_pos, first, neg_fill)
                second = jnp.where(k_pos + half <= q_pos, second, neg_fill)
            old_max = row_max[0:1, span]
            top = jnp.maximum(
                jnp.max(first, axis=0, keepdims=True), jnp.max(second, axis=0, keepdims=True)
            )
            new_max = jnp.maximum(old_max, top)
            probs = jnp.concatenate(
                [
                    jnp.exp2((first - new_max) * LOG2E).astype(jnp.bfloat16),
                    jnp.exp2((second - new_max) * LOG2E).astype(jnp.bfloat16),
                ],
                axis=0,
            )
            keep = jnp.exp2((old_max - new_max) * LOG2E)
            acc[:, span] = acc[:, span] * keep + dot(values, probs)
            row_max[0:1, span] = new_max

    block_step(me, kv_ref, True)

    high = weight_ref[...].astype(jnp.bfloat16)
    low = (weight_ref[...] - high.astype(jnp.float32)).astype(jnp.bfloat16)
    for start in range(0, slot_count, slot_tile):
        span = slice(start, start + slot_tile)
        match = dot_nt(ranks, places_ref[span, :])
        for index, part in enumerate((high, low)):
            value = dot_nt(part, places_ref[span, 0:LANES])
            spread[index, :, span] = jnp.where(match == 0.0, value, 0.0).astype(jnp.bfloat16)
    shared = silu(dot_nt(shared_gate_ref[...], normed_ref[...])) * dot_nt(
        shared_up_ref[...], normed_ref[...]
    )
    hidden_out[...] = jnp.zeros_like(hidden_out)
    hidden_out[:, slot_span : slot_span + tokens] = shared.astype(jnp.bfloat16)

    def choose(parts, span):
        owner = owner_ref[0:1, span]
        value = parts[0]
        for index in range(1, experts):
            value = jnp.where(owner == float(index), parts[index], value)
        return value

    def gather_stage():
        loop(ep_count - 1, lambda turn: pick_copy(ep_at(turn), ep_at(turn)).wait_recv())
        own_pick().wait()
        loop(tall - 1, lambda turn: piece_copy(y_at(turn), y_me).start())

    def parts_stage():
        loop(tall - 1, lambda turn: piece_copy(y_at(turn), y_at(turn)).wait_recv())

        def wait_weights(turn):
            weight_copy(gate_w, 0, x_at(turn), x_at(turn)).wait_recv()
            weight_copy(up_w, 1, x_at(turn), x_at(turn)).wait_recv()

        loop(wide - 1, wait_weights)
        own_weight(gate_w, 0).wait()
        own_weight(up_w, 1).wait()

        def one_target(turn):
            target = lax.rem(x_me + turn, wide)
            block = weights[target].reshape(2 * experts * own_hidden, features)
            for start in range(0, slot_count, slot_tile):
                span = slice(start, start + slot_tile)
                rows_of = jnp.concatenate([pieces[y, span, :] for y in range(tall)], axis=1)
                full = dot_nt(block, rows_of)
                halves = []
                for index in range(2):
                    base = index * experts * own_hidden
                    halves.append(
                        choose(
                            [
                                full[base + e * own_hidden : base + (e + 1) * own_hidden]
                                for e in range(experts)
                            ],
                            span,
                        )
                    )
                part_out[target, :, span] = jnp.concatenate(halves, axis=0).astype(jnp.bfloat16)

        loop(wide, one_target)
        loop(wide - 1, lambda turn: part_copy(x_at(turn), x_me).start())

    def hidden_stage():
        loop(wide - 1, lambda turn: part_copy(x_at(turn), x_at(turn)).wait_recv())
        total = part_out[x_me].astype(jnp.float32)
        for turn in range(wide - 1):
            total = total + part_in[x_at(turn)].astype(jnp.float32)
        hidden = silu(total[0:own_hidden]) * total[own_hidden:]
        hidden_out[:, 0:slot_count] = hidden.astype(jnp.bfloat16)
        hidden_all[tp_me] = hidden_out[...]
        loop(tp_count - 1, lambda turn: hidden_copy(tp_at(turn), tp_me).start())

    def down_stage():
        loop(tp_count - 1, lambda turn: hidden_copy(tp_at(turn), tp_at(turn)).wait_recv())
        for start in range(0, slot_count, slot_tile):
            span = slice(start, start + slot_tile)
            units = hidden_all[:, :, span].reshape(tp_count * own_hidden, slot_tile)
            results = [dot(down_ref[e], units) for e in range(experts)]
            result_out[span, :] = choose(results, span).T.astype(jnp.bfloat16)
        loop(ep_count - 1, lambda turn: result_copy(ep_at(turn), me).start())
        own_result().start()

    def received(hop, downward):
        going_up = jnp.logical_and(hop >= 1, jnp.logical_and(hop <= up_hops, chip - hop >= 0))
        source = lax.rem(chip + hop, chips)
        going_down = jnp.logical_and(
            hop >= 1, jnp.logical_and(hop <= down_hops, source <= last_down)
        )
        return jnp.where(downward, going_down, going_up)

    def useful(hop, downward):
        return jnp.logical_and(
            received(hop, downward), jnp.logical_or(jnp.logical_not(downward), chip + hop >= chips)
        )

    def forwards_up(hop):
        return jnp.logical_and(
            received(hop, False), jnp.logical_and(hop < up_hops, chip < chips - 1)
        )

    def forwards_down(hop):
        return jnp.logical_and(received(hop, True), hop < down_hops)

    def home_of(hop, downward):
        return jnp.where(downward, lax.rem(chip + hop, chips), chip - hop)

    def substep(index):
        hop = index // 4
        kind = index % 4
        downward = kind % 2 == 1
        own_core = kind < 2
        home = home_of(hop, downward)
        slot = home * CORES + jnp.where(own_core, core, other)
        sibling = jnp.logical_and(index == 2, core == 1)
        used = useful(hop, downward)

        @pl.when(jnp.logical_and(own_core, received(hop, downward)))
        def _():
            up_copy(held.at[slot], slot).wait_recv()

        @pl.when(jnp.logical_and(kind == 0, forwards_up(hop)))
        def _():
            up_copy(held.at[slot], slot).start()

        @pl.when(jnp.logical_and(kind == 1, forwards_down(hop)))
        def _():
            down_copy(held.at[slot], slot).start()

        @pl.when(jnp.logical_and(own_core, used))
        def _():
            side_copy(held.at[slot], slot).start()

        @pl.when(jnp.logical_or(jnp.logical_and(jnp.logical_not(own_core), used), sibling))
        def _():
            side_copy(held.at[slot], slot).wait_recv()

        @pl.when(jnp.logical_or(used, sibling))
        def _():
            block_step(slot, held.at[slot], False)

        pl.when(index == GATHER_AT)(gather_stage)
        pl.when(index == PARTS_AT)(parts_stage)
        pl.when(index == HIDDEN_AT)(hidden_stage)
        pl.when(index == DOWN_AT)(down_stage)

    loop(max(4 * up_hops + 4, DOWN_AT + 1), substep, 2)

    heads_out[...] = (acc[0:HEAD] / acc[HEAD : HEAD + 1]).astype(jnp.bfloat16)
    heads_all[tp_me] = heads_out[...]
    loop(tp_count - 1, lambda turn: head_copy(tp_at(turn), tp_me).start())

    loop(ep_count - 1, lambda turn: result_copy(ep_at(turn), ep_at(turn)).wait_recv())
    own_result().wait()
    shared_units = hidden_all[:, :, slot_span:].reshape(tp_count * own_hidden, -1)
    shared_sum = dot(shared_down_ref[...], shared_units).T[0:tokens]
    routed = dot(spread[0], result_in[...]) + dot(spread[1], result_in[...])
    moe_ref[...] = (routed + shared_sum).astype(moe_ref.dtype)

    def finish_ep(turn):
        pick_copy(ep_at(turn), me).wait_send()
        result_copy(ep_at(turn), me).wait_send()

    loop(ep_count - 1, finish_ep)
    loop(tall - 1, lambda turn: piece_copy(y_at(turn), y_me).wait_send())

    def finish_x(turn):
        weight_copy(gate_w, 0, x_at(turn), x_me).wait_send()
        weight_copy(up_w, 1, x_at(turn), x_me).wait_send()
        part_copy(x_at(turn), x_me).wait_send()

    loop(wide - 1, finish_x)
    loop(tp_count - 1, lambda turn: hidden_copy(tp_at(turn), tp_me).wait_send())

    @pl.when(chip < chips - 1)
    def _():
        up_copy(kv_ref, me).wait_send()

    @pl.when(chip <= last_down)
    def _():
        down_copy(kv_ref, me).wait_send()

    @pl.when(core == 0)
    def _():
        side_copy(kv_ref, me).wait_send()

    def finish_hop(hop):
        low_slot = home_of(hop, False) * CORES + core
        high_slot = home_of(hop, True) * CORES + core

        @pl.when(forwards_up(hop))
        def _():
            up_copy(held.at[low_slot], low_slot).wait_send()

        @pl.when(forwards_down(hop))
        def _():
            down_copy(held.at[high_slot], high_slot).wait_send()

        @pl.when(useful(hop, False))
        def _():
            side_copy(held.at[low_slot], low_slot).wait_send()

        @pl.when(useful(hop, True))
        def _():
            side_copy(held.at[high_slot], high_slot).wait_send()

    loop(up_hops + 1, finish_hop, 1)

    loop(tp_count - 1, lambda turn: head_copy(tp_at(turn), tp_at(turn)).wait_recv())
    for start in range(0, rows, tile):
        span = slice(start, start + tile)
        units = heads_all[:, :, span].reshape(tp_count * HEAD, tile)
        mixed = dot(out_weight_ref[...], units)
        mixer_ref[span, :] = mixed.T.astype(mixer_ref.dtype)
    loop(tp_count - 1, lambda turn: head_copy(tp_at(turn), tp_me).wait_send())


def slot_tables(ep_count, experts, cap, room):
    slot = np.arange(ep_count * room)
    inside = slot % room
    real = inside < experts * cap
    places = np.zeros((slot.size, 2 * LANES), np.float32)
    expert = (slot // room) * experts + inside // cap
    places[slot[real], expert[real]] = 1.0
    places[:, LANES] = np.where(real, -(inside % cap), 5.0)
    owner = np.where(real, inside // cap, 0).astype(np.float32)
    return jnp.asarray(places, jnp.bfloat16), jnp.asarray(np.tile(owner, (8, 1)), jnp.float32)


def local(
    query_rows,
    key_rows,
    value_rows,
    cum_gate,
    out_weight,
    moe_input,
    moe_gain,
    routes,
    route_weight,
    expert_gate,
    expert_up,
    expert_down,
    shared_gate,
    shared_up,
    shared_down,
):
    rows, width = query_rows.shape
    half = rows // 2
    chunks = rows // LANES
    token_count = moe_input.shape[0]
    top_count = routes.shape[1]
    experts, model, own_hidden = expert_gate.shape
    ep_count = lax.axis_size("ep")
    tp_count = lax.axis_size("tp")
    wide, tall = plane_shape(tp_count)
    expert_count = experts * ep_count
    cap = 2 * token_count * top_count // expert_count
    room = -(-experts * cap // 8) * 8
    slot_count = ep_count * room
    slot_span = -(-slot_count // LANES) * LANES
    hidden_span = slot_span + -(-token_count // LANES) * LANES
    columns = expert_down.shape[2]

    moe_rows = moe_input.astype(jnp.float32)
    normed = (
        moe_rows
        * lax.rsqrt(jnp.mean(moe_rows * moe_rows, axis=1, keepdims=True) + norm_eps)
        * moe_gain
    ).astype(jnp.bfloat16)
    expert_ids = jnp.arange(LANES, dtype=jnp.int32)
    chosen = routes[:, :, None] == expert_ids[None, None, :]
    named = jnp.any(chosen, axis=1)
    weight_of = jnp.sum(jnp.where(chosen, route_weight[:, :, None], 0.0), axis=1)
    order = jnp.arange(token_count)
    earlier = (order[None, :] < order[:, None]).astype(jnp.bfloat16)
    ranks = jnp.dot(earlier, named.astype(jnp.bfloat16), preferred_element_type=jnp.float32)
    ranks = jnp.where(named, ranks, -1.0).astype(jnp.bfloat16)

    queries = query_rows.T * jnp.asarray(HEAD**-0.5, jnp.bfloat16)
    value_cols = value_rows.T
    key_value = jnp.concatenate(
        [jnp.concatenate([key_rows[:half], key_rows[half:]], axis=1)]
        + [value_cols[:, LANES * i : LANES * (i + 1)] for i in range(chunks)],
        axis=0,
    )
    minus = -cum_gate.reshape(ep_count, rows)
    first = lax.reduce_precision(minus, 8, 7)
    rest = minus - first
    second = lax.reduce_precision(rest, 8, 7)
    third = rest - second
    terms = jnp.stack([first, second, third, jnp.zeros_like(third)], axis=1).astype(jnp.bfloat16)
    terms = terms.reshape(ep_count * TERMS, rows)
    terms = jnp.pad(terms, ((0, LANES - ep_count * TERMS), (0, 0))).T

    places, owner = slot_tables(ep_count, experts, cap, room)
    dma = pltpu.SemaphoreType.DMA
    vmem = pl.BlockSpec(memory_space=pltpu.VMEM)
    anywhere = pl.BlockSpec(memory_space=pl.ANY)
    blocks = ep_count * rows * rows
    bf16 = jnp.bfloat16
    mixer_out, moe_out = pl.pallas_call(
        functools.partial(layer_kernel, cap, room),
        out_shape=[
            jax.ShapeDtypeStruct((rows, columns), bf16),
            jax.ShapeDtypeStruct((token_count, columns), bf16),
        ],
        in_specs=[vmem] * 8 + [anywhere] * 2 + [vmem] * 5,
        out_specs=[vmem, vmem],
        scratch_shapes=[
            pltpu.VMEM((ep_count, rows, LANES), bf16),
            pltpu.VMEM((HEAD + 16, rows), jnp.float32),
            pltpu.VMEM((8, rows), jnp.float32),
            pltpu.VMEM((slot_count, LANES), bf16),
            pltpu.VMEM((tall, slot_count, LANES), bf16),
            pltpu.VMEM((wide, 2, experts, own_hidden, model // wide), bf16),
            pltpu.VMEM((wide, 2 * own_hidden, slot_count), bf16),
            pltpu.VMEM((wide, 2 * own_hidden, slot_count), bf16),
            pltpu.VMEM((own_hidden, hidden_span), bf16),
            pltpu.VMEM((tp_count, own_hidden, hidden_span), bf16),
            pltpu.VMEM((slot_count, columns), bf16),
            pltpu.VMEM((slot_count, columns), bf16),
            pltpu.VMEM((2, token_count, slot_count), bf16),
            pltpu.VMEM((HEAD, rows), bf16),
            pltpu.VMEM((tp_count, HEAD, rows), bf16),
        ]
        + [dma((ep_count,))] * 8
        + [dma((tall,))] * 2
        + [dma((2, wide))] * 2
        + [dma((wide,))] * 2
        + [dma((tp_count,))] * 4
        + [dma((4,))],
        compiler_params=pltpu.CompilerParams(
            collective_id=0, has_side_effects=True, vmem_limit_bytes=56 * 1024 * 1024
        ),
        cost_estimate=pl.CostEstimate(
            flops=blocks * 2 * 512, bytes_accessed=8 * 1024 * 1024, transcendentals=blocks
        ),
        name="layer",
    )(
        queries,
        key_value,
        terms,
        normed,
        ranks,
        weight_of,
        places,
        owner,
        expert_gate.transpose(0, 2, 1),
        expert_up.transpose(0, 2, 1),
        expert_down.transpose(0, 2, 1),
        shared_gate.T,
        shared_up.T,
        shared_down.T,
        out_weight.T,
    )
    return mixer_out, moe_out


def solution(mesh):
    placed = (
        P("ep", "tp"),
        P("ep", "tp"),
        P("ep", "tp"),
        P("tp", None),
        P(None, "tp"),
        P("ep", None),
        P(),
        P("ep", None),
        P("ep", None),
        P("ep", None, "tp"),
        P("ep", None, "tp"),
        P("ep", None, "tp"),
        P(None, "tp"),
        P(None, "tp"),
        P(None, "tp"),
    )
    return jax.shard_map(
        local, mesh=mesh, in_specs=placed, out_specs=(P("ep", "tp"), P("ep", "tp")), check_vma=False
    )
```

time: 433 us -> 151 us (0.35)
  the two profiles are of different devices: /device:TPU:1 before, /device:TPU:464 now
where the time goes in v1:
time: 151 us
  Pallas kernels  138 us (91%)
  local copies, waits for them, and re-layouts  7.18 us (5%)
  other arithmetic  4.64 us (3%)
    pallas_call x1, Pallas kernels, local(): pl.pallas_call(functools.partial(layer_kernel, cap, room), out_shape=[jax...  138 us
    unnamed x36, local copies, waits for them, and re-layouts  6.04 us

profile of v1, /device:TPU:464, one launch (start us, length us, event | category | flops | bytes accessed | tf_op | source)
XLA Modules:
  0.0 151.0 jit_solution(1401692043882285022)
XLA Ops:
  0.6 0.0 copy-start.9
  0.6 0.0 copy-start.5
  0.6 0.0 copy-start.4
  0.7 0.1 pad.3.clone
  0.7 1.4 fusion
  2.1 0.0 copy-done.9
  2.1 0.1 fusion.4
  2.3 0.8 fusion.3.ranks_ref
  3.1 0.0 copy-done.4
  3.1 0.6 multiply_bitcast_fusion.q_ref
  3.7 0.0 copy-done.5
  3.7 0.3 negate_reduce_fusion
  4.1 0.0 copy-start.11
  4.1 0.0 copy-start.6
  4.1 0.1 maximum_maximum_fusion
  4.2 0.2 copy.48
  4.3 0.0 copy-start.7
  4.3 0.1 convert_element_type.16
  4.4 0.0 copy-start.3
  4.4 0.0 copy-start.2
  4.4 0.8 copy.49
  5.2 0.0 copy-done.11
  5.2 0.9 select_reduce_fusion.weight_ref
  6.1 0.0 copy-done.6
  6.1 0.0 copy-start.1
  6.1 0.1 copy.53
  6.3 0.1 copy.54
  6.4 0.1 maximum_dynamic-update-slice_fusion
  6.5 0.0 copy-done.7
  6.6 0.0 copy-done.3
  6.6 0.0 copy-start.8
  6.6 0.8 copy.51
  7.4 0.0 copy-done.2
  7.4 0.0 copy-start
  7.4 0.0 copy-start.10
  7.4 0.9 copy.52
  8.2 0.0 copy-done.1
  8.3 1.0 copy.50
  9.3 0.0 copy-done.8
  9.3 0.0 copy-done
  9.3 0.0 copy-done.10
  9.3 1.1 fusion.2.normed_ref
  10.4 137.6 %layer.1 = (bf16[768,128]{1,0:T(8,128)(2,1)}, bf16[192,128]{1,0:T(8,128)(2,1)}) custom-call(bf16[64,768]{1,0:T(8,128)(2,1)} %multiply_bitcast_fusion.q_ref, bf16[768,128]{1,0:T(8,128)(2,1)} %copy-done.8, bf16[768,128]{1,0:T(8,128)(2,1)} %bitcast.15, bf16[192,2048]{1,0:T(8,128)(2,1)} %fusion.2.normed_ref, bf16[192,128]{1,0:T(8,128)(2,1)} %fusion.3.ranks_ref, ...), custom_call_target="tpu_custom_call" | custom-call | flops 19327352832 | bytes 8388608 | tf_op jit(solution)/shard_map/layer/pallas_call | solution.py:646
  148.0 1.6 %copy.63 = bf16[768,128]{1,0:T(8,128)(2,1)} copy(bf16[768,128]{1,0:T(8,128)(2,1)} %get-tuple-element.9) | data formatting | bytes 393216
  149.6 1.4 copy.64
  (10 shorter events, 0.1 us)
Async XLA Ops:
  0.6 1.5 copy-start.9
  0.6 3.1 %copy-start.5 = (f32[1,24576]{1,0:T(1,128)S(1)}, f32[1,24576]{1,0:T(1,128)}, u32[]{:S(2)}) copy-start(f32[1,24576]{1,0:T(1,128)} %param.20) | copy-start | bytes 294916
  0.6 2.4 %copy-start.4 = (bf16[768,64]{0,1:T(8,128)(2,1)S(1)}, bf16[768,64]{0,1:T(8,128)(2,1)}, u32[]{:S(2)}) copy-start(bf16[768,64]{0,1:T(8,128)(2,1)} %param.17) | copy-start | bytes 294916
  4.1 1.2 copy-start.11
  4.1 2.0 %copy-start.6 = (bf16[768,64]{0,1:T(8,128)(2,1)S(1)}, bf16[768,64]{0,1:T(8,128)(2,1)}, u32[]{:S(2)}) copy-start(bf16[768,64]{0,1:T(8,128)(2,1)} %param.18) | copy-start | bytes 294916
  4.3 2.2 %copy-start.7 = (bf16[768,64]{0,1:T(8,128)(2,1)S(1)}, bf16[768,64]{0,1:T(8,128)(2,1)}, u32[]{:S(2)}) copy-start(bf16[768,64]{0,1:T(8,128)(2,1)} %param.19) | copy-start | bytes 294916
  4.4 2.2 %copy-start.3 = (bf16[512,128]{1,0:T(8,128)(2,1)S(1)}, bf16[512,128]{1,0:T(8,128)(2,1)}, u32[]{:S(2)}) copy-start(bf16[512,128]{1,0:T(8,128)(2,1)} %param.31) | copy-start | bytes 393220
  4.4 3.0 %copy-start.2 = (bf16[1024,128]{1,0:T(8,128)(2,1)S(1)}, bf16[1024,128]{1,0:T(8,128)(2,1)}, u32[]{:S(2)}) copy-start(bf16[1024,128]{1,0:T(8,128)(2,1)} %param.21) | copy-start | bytes 786436
  6.1 2.1 %copy-start.1 = (bf16[4,512,128]{2,1,0:T(8,128)(2,1)S(1)}, bf16[4,512,128]{2,1,0:T(8,128)(2,1)}, u32[]{:S(2)}) copy-start(bf16[4,512,128]{2,1,0:T(8,128)(2,1)} %param.28) | copy-start | bytes 1572868
  6.6 2.7 %copy-start.8 = (bf16[768,128]{1,0:T(8,128)(2,1)}, bf16[768,128]{1,0:T(8,128)(2,1)S(1)}, u32[]{:S(2)}) copy-start(bf16[768,128]{1,0:T(8,128)(2,1)S(1)} %slice_dynamic-update-slice_fusion.kv_ref) | copy-start | bytes 589828
  7.4 1.9 %copy-start = (bf16[192,2048]{1,0:T(8,128)(2,1)S(1)}, bf16[192,2048]{1,0:T(8,128)(2,1)}, u32[]{:S(2)}) copy-start(bf16[192,2048]{1,0:T(8,128)(2,1)} %param.22) | copy-start | bytes 2359300
  7.4 1.9 %copy-start.10 = (f32[2048]{0:T(1024)S(1)}, f32[2048]{0:T(1024)}, u32[]{:S(2)}) copy-start(f32[2048]{0:T(1024)} %param.23) | copy-start | bytes 24580

commit v2 on v1

--- a/solution.py
+++ b/solution.py
@@ -17,10 +17,12 @@
 neg_fill = -1e30
 norm_eps = 1e-06
 
-GATHER_AT = 10
-PARTS_AT = 16
-HIDDEN_AT = 20
-DOWN_AT = 26
+NEAR_AT = 7
+FAR_AT = 9
+PARTS_AT = 17
+HIDDEN_AT = 24
+DOWN_AT = 27
+RETURN_AT = 31
 
 
 def plane_shape(tp_count):
@@ -63,7 +65,7 @@
     owner_ref,
     gate_w,
     up_w,
-    down_ref,
+    down_w,
     shared_gate_ref,
     shared_up_ref,
     shared_down_ref,
@@ -76,14 +78,16 @@
     picked,
     pieces,
     weights,
+    down_all,
     part_out,
     part_in,
-    hidden_out,
     hidden_all,
+    shared_out,
+    shared_all,
     result_out,
+    result_all,
     result_in,
     spread,
-    heads_out,
     heads_all,
     up_send,
     down_send,
@@ -93,6 +97,8 @@
     pick_recv,
     result_send,
     result_recv,
+    cross_send,
+    cross_recv,
     piece_send,
     piece_recv,
     weight_send,
@@ -101,7 +107,10 @@
     part_recv,
     hidden_send,
     hidden_recv,
-    head_send,
+    shared_send,
+    shared_recv,
+    row_send,
+    column_send,
     head_recv,
     own_sem,
 ):
@@ -114,7 +123,6 @@
     own_hidden = gate_w.shape[1]
     slot_count = picked.shape[0]
     slot_tile = 256 if slot_count % 256 == 0 else slot_count
-    slot_span = -(-slot_count // LANES) * LANES
 
     me = lax.axis_index("ep")
     ep_count = lax.axis_size("ep")
@@ -131,6 +139,9 @@
     down_hops = chips - 1 - up_hops
     last_down = chips - 2 - up_hops
     features = normed_ref.shape[1] // wide
+    share = ep_count // wide
+    share_rows = share * room
+    keeper = me // share
 
     def ep_at(turn):
         return lax.rem(me + turn + 1, ep_count)
@@ -184,18 +195,27 @@
             device_id={"ep": target},
         )
 
-    def weight_copy(source, index, target, owner):
-        return pltpu.make_async_remote_copy(
-            src_ref=source.at[:, :, feature_lanes(target)],
-            dst_ref=weights.at[owner, index],
+    sources = (
+        (gate_w.at[:, :, feature_lanes(x_me)], lambda owner: weights.at[0, :, owner]),
+        (up_w.at[:, :, feature_lanes(x_me)], lambda owner: weights.at[1, :, owner]),
+        (down_w, lambda owner: down_all.at[owner]),
+    )
+
+    def weight_copy(index, target, owner):
+        source = down_w
+        if index < 2:
+            source = (gate_w, up_w)[index].at[:, :, feature_lanes(target)]
+        return pltpu.make_async_remote_copy(
+            src_ref=source,
+            dst_ref=sources[index][1](owner),
             send_sem=weight_send.at[index, target],
             recv_sem=weight_recv.at[index, owner],
             device_id={"tp": y_me * wide + target},
         )
 
-    def own_weight(source, index):
+    def own_weight(index):
         return pltpu.make_async_copy(
-            source.at[:, :, feature_lanes(x_me)], weights.at[x_me, index], own_sem.at[index]
+            sources[index][0], sources[index][1](x_me), own_sem.at[index]
         )
 
     def up_copy(src, slot):
@@ -225,18 +245,19 @@
             device_id={"ep": chip * CORES + other},
         )
 
-    def piece_copy(target, owner):
-        return pltpu.make_async_remote_copy(
-            src_ref=pieces.at[owner],
-            dst_ref=pieces.at[owner],
-            send_sem=piece_send.at[target],
-            recv_sem=piece_recv.at[owner],
+    def piece_copy(group, target, owner):
+        place = pieces.at[owner, pl.ds(pl.multiple_of(group * share_rows, 8), share_rows)]
+        return pltpu.make_async_remote_copy(
+            src_ref=place,
+            dst_ref=place,
+            send_sem=piece_send.at[target, group],
+            recv_sem=piece_recv.at[owner, group],
             device_id={"tp": target * wide + x_me},
         )
 
     def part_copy(target, owner):
         return pltpu.make_async_remote_copy(
-            src_ref=part_out.at[target],
+            src_ref=part_out.at[pl.ds(pl.multiple_of(target * share_rows, 8), share_rows)],
             dst_ref=part_in.at[owner],
             send_sem=part_send.at[target],
             recv_sem=part_recv.at[owner],
@@ -245,16 +266,42 @@
 
     def hidden_copy(target, owner):
         return pltpu.make_async_remote_copy(
-            src_ref=hidden_out,
+            src_ref=hidden_all.at[owner],
             dst_ref=hidden_all.at[owner],
             send_sem=hidden_send.at[target],
             recv_sem=hidden_recv.at[owner],
+            device_id={"tp": target * wide + x_me},
+        )
+
+    def shared_copy(target, owner):
+        return pltpu.make_async_remote_copy(
+            src_ref=shared_out,
+            dst_ref=shared_all.at[owner],
+            send_sem=shared_send.at[target],
+            recv_sem=shared_recv.at[owner],
             device_id={"tp": target},
         )
 
+    def share_of(index):
+        return pl.ds(pl.multiple_of(index * share_rows, 8), share_rows)
+
+    def cross_copy(target, owner):
+        return pltpu.make_async_remote_copy(
+            src_ref=result_out.at[target],
+            dst_ref=result_all.at[share_of(owner)],
+            send_sem=cross_send.at[target],
+            recv_sem=cross_recv.at[owner],
+            device_id={"tp": y_me * wide + target},
+        )
+
+    def own_cross():
+        return pltpu.make_async_copy(
+            result_out.at[x_me], result_all.at[share_of(x_me)], own_sem.at[5]
+        )
+
     def result_copy(target, owner):
         return pltpu.make_async_remote_copy(
-            src_ref=result_out.at[room_of(target)],
+            src_ref=result_all.at[room_of(target)],
             dst_ref=result_in.at[room_of(owner)],
             send_sem=result_send.at[target],
             recv_sem=result_recv.at[owner],
@@ -263,26 +310,48 @@
 
     def own_result():
         return pltpu.make_async_copy(
-            result_out.at[room_of(me)], result_in.at[room_of(me)], own_sem.at[2]
-        )
-
-    def head_copy(target, owner):
-        return pltpu.make_async_remote_copy(
-            src_ref=heads_out,
-            dst_ref=heads_all.at[owner],
-            send_sem=head_send.at[target],
-            recv_sem=head_recv.at[owner],
-            device_id={"tp": target},
-        )
+            result_all.at[room_of(me)], result_in.at[room_of(me)], own_sem.at[4]
+        )
+
+    half_head = HEAD // 2
+
+    def row_copy(owner_y, owner_x, part, target, sem):
+        place = heads_all.at[owner_y, owner_x, part * half_head : (part + 1) * half_head]
+        return pltpu.make_async_remote_copy(
+            src_ref=place,
+            dst_ref=place,
+            send_sem=sem,
+            recv_sem=head_recv.at[part, owner_y * wide + owner_x],
+            device_id={"tp": y_me * wide + target},
+        )
+
+    def column_copy(owner_y, owner_x, part, target, sem):
+        place = heads_all.at[owner_y, owner_x, part * half_head : (part + 1) * half_head]
+        return pltpu.make_async_remote_copy(
+            src_ref=place,
+            dst_ref=place,
+            send_sem=sem,
+            recv_sem=head_recv.at[part, owner_y * wide + owner_x],
+            device_id={"tp": target * wide + x_me},
+        )
+
+    def row_part(owner_x, target):
+        return column_copy(y_me, owner_x, 0, target, column_send.at[0, owner_x, target])
+
+    def row_first(target, owner_x):
+        return row_copy(y_me, owner_x, 0, target, row_send.at[1, tall, target])
+
+    def column_part(owner_y, target):
+        return row_copy(owner_y, x_me, 1, target, row_send.at[0, owner_y, target])
+
+    def column_first(target, owner_y):
+        return column_copy(owner_y, x_me, 1, target, column_send.at[1, wide, target])
 
     def own_pick():
         return pltpu.make_async_copy(
             picked.at[room_of(me)], pieces.at[y_me, room_of(me)], own_sem.at[3]
         )
 
-    loop(ep_count - 1, lambda turn: pick_copy(ep_at(turn), me).start())
-    own_pick().start()
-
     @pl.when(chip < chips - 1)
     def _():
         up_copy(kv_ref, me).start()
@@ -295,13 +364,14 @@
     def _():
         side_copy(kv_ref, me).start()
 
-    def start_weights(turn):
-        weight_copy(gate_w, 0, x_at(turn), x_me).start()
-        weight_copy(up_w, 1, x_at(turn), x_me).start()
-
-    loop(wide - 1, start_weights)
-    own_weight(gate_w, 0).start()
-    own_weight(up_w, 1).start()
+    loop(ep_count - 1, lambda turn: pick_copy(ep_at(turn), me).start())
+    own_pick().start()
+
+    loop(wide - 1, lambda turn: weight_copy(0, x_at(turn), x_me).start())
+    loop(wide - 1, lambda turn: weight_copy(1, x_at(turn), x_me).start())
+    for index in range(3):
+        own_weight(index).start()
+    loop(wide - 1, lambda turn: weight_copy(2, x_at(turn), x_me).start())
 
     ones = jnp.ones((acc.shape[0] - HEAD, rows), jnp.bfloat16)
     nothing = jnp.zeros((HEAD, tile), jnp.bfloat16)
@@ -356,73 +426,92 @@
     shared = silu(dot_nt(shared_gate_ref[...], normed_ref[...])) * dot_nt(
         shared_up_ref[...], normed_ref[...]
     )
-    hidden_out[...] = jnp.zeros_like(hidden_out)
-    hidden_out[:, slot_span : slot_span + tokens] = shared.astype(jnp.bfloat16)
+    shared_out[...] = jnp.zeros_like(shared_out)
+    shared_out[:, 0:tokens] = shared.astype(jnp.bfloat16)
+    shared_all[tp_me] = shared_out[...]
+    loop(tp_count - 1, lambda turn: shared_copy(tp_at(turn), tp_me).start())
 
     def choose(parts, span):
-        owner = owner_ref[0:1, span]
+        owner = owner_ref[span, 0:1]
         value = parts[0]
         for index in range(1, experts):
             value = jnp.where(owner == float(index), parts[index], value)
         return value
 
-    def gather_stage():
-        loop(ep_count - 1, lambda turn: pick_copy(ep_at(turn), ep_at(turn)).wait_recv())
+    def forward_group(group):
+        def wait_block(turn):
+            source = group * share + turn
+
+            @pl.when(source != me)
+            def _():
+                pick_copy(source, source).wait_recv()
+
+        loop(share, wait_block)
+        loop(tall - 1, lambda turn: piece_copy(group, y_at(turn), y_me).start())
+
+    def near_stage():
         own_pick().wait()
-        loop(tall - 1, lambda turn: piece_copy(y_at(turn), y_me).start())
+        forward_group(keeper)
+
+    def far_stage():
+        loop(wide, lambda turn: forward_group(lax.rem(keeper + turn, wide)), 1)
 
     def parts_stage():
-        loop(tall - 1, lambda turn: piece_copy(y_at(turn), y_at(turn)).wait_recv())
-
-        def wait_weights(turn):
-            weight_copy(gate_w, 0, x_at(turn), x_at(turn)).wait_recv()
-            weight_copy(up_w, 1, x_at(turn), x_at(turn)).wait_recv()
-
-        loop(wide - 1, wait_weights)
-        own_weight(gate_w, 0).wait()
-        own_weight(up_w, 1).wait()
-
-        def one_target(turn):
-            target = lax.rem(x_me + turn, wide)
-            block = weights[target].reshape(2 * experts * own_hidden, features)
-            for start in range(0, slot_count, slot_tile):
-                span = slice(start, start + slot_tile)
-                rows_of = jnp.concatenate([pieces[y, span, :] for y in range(tall)], axis=1)
-                full = dot_nt(block, rows_of)
-                halves = []
-                for index in range(2):
-                    base = index * experts * own_hidden
-                    halves.append(
-                        choose(
-                            [
-                                full[base + e * own_hidden : base + (e + 1) * own_hidden]
-                                for e in range(experts)
-                            ],
-                            span,
-                        )
-                    )
-                part_out[target, :, span] = jnp.concatenate(halves, axis=0).astype(jnp.bfloat16)
-
-        loop(wide, one_target)
+        def wait_pieces(group):
+            loop(tall - 1, lambda turn: piece_copy(group, y_at(turn), y_at(turn)).wait_recv())
+
+        loop(wide, wait_pieces)
+        for index in range(2):
+            loop(wide - 1, lambda turn: weight_copy(index, x_at(turn), x_at(turn)).wait_recv())
+            own_weight(index).wait()
+
+        def one_tile(index):
+            start = pl.multiple_of(index * slot_tile, slot_tile)
+            span = pl.ds(start, slot_tile)
+            rows_of = jnp.concatenate([pieces[y, span, :] for y in range(tall)], axis=1)
+            parts = []
+            for e in range(experts):
+                block = jnp.concatenate(
+                    [weights[g, e].reshape(wide * own_hidden, features) for g in range(2)], axis=0
+                )
+                parts.append(dot_nt(rows_of, block))
+            part_out[span, :] = choose(parts, span).astype(jnp.bfloat16)
+
+        loop(slot_count // slot_tile, one_tile)
         loop(wide - 1, lambda turn: part_copy(x_at(turn), x_me).start())
 
     def hidden_stage():
         loop(wide - 1, lambda turn: part_copy(x_at(turn), x_at(turn)).wait_recv())
-        total = part_out[x_me].astype(jnp.float32)
+        own_rows = pl.ds(pl.multiple_of(x_me * share_rows, 8), share_rows)
+        total = part_out[own_rows, :].astype(jnp.float32)
         for turn in range(wide - 1):
             total = total + part_in[x_at(turn)].astype(jnp.float32)
-        hidden = silu(total[0:own_hidden]) * total[own_hidden:]
-        hidden_out[:, 0:slot_count] = hidden.astype(jnp.bfloat16)
-        hidden_all[tp_me] = hidden_out[...]
-        loop(tp_count - 1, lambda turn: hidden_copy(tp_at(turn), tp_me).start())
+        middle = wide * own_hidden
+        hidden = silu(total[:, 0:middle]) * total[:, middle:]
+        hidden_all[y_me] = hidden.astype(jnp.bfloat16)
+        loop(tall - 1, lambda turn: hidden_copy(y_at(turn), y_me).start())
 
     def down_stage():
-        loop(tp_count - 1, lambda turn: hidden_copy(tp_at(turn), tp_at(turn)).wait_recv())
-        for start in range(0, slot_count, slot_tile):
-            span = slice(start, start + slot_tile)
-            units = hidden_all[:, :, span].reshape(tp_count * own_hidden, slot_tile)
-            results = [dot(down_ref[e], units) for e in range(experts)]
-            result_out[span, :] = choose(results, span).T.astype(jnp.bfloat16)
+        loop(tall - 1, lambda turn: hidden_copy(y_at(turn), y_at(turn)).wait_recv())
+        loop(wide - 1, lambda turn: weight_copy(2, x_at(turn), x_at(turn)).wait_recv())
+        own_weight(2).wait()
+        units = jnp.concatenate([hidden_all[y] for y in range(tall)], axis=1)
+        for x in range(0, wide, 2):
+            results = [
+                dot(units, jnp.concatenate([down_all[x, e], down_all[x + 1, e]], axis=1))
+                for e in range(experts)
+            ]
+            result = choose(results, slice(0, share_rows)).astype(jnp.bfloat16)
+            columns = result.shape[1] // 2
+            result_out[x] = result[:, 0:columns]
+            result_out[x + 1] = result[:, columns:]
+
+        loop(wide - 1, lambda turn: cross_copy(x_at(turn), x_me).start())
+        own_cross().start()
+
+    def return_stage():
+        loop(wide - 1, lambda turn: cross_copy(x_at(turn), x_at(turn)).wait_recv())
+        own_cross().wait()
         loop(ep_count - 1, lambda turn: result_copy(ep_at(turn), me).start())
         own_result().start()
 
@@ -450,32 +539,37 @@
     def home_of(hop, downward):
         return jnp.where(downward, lax.rem(chip + hop, chips), chip - hop)
 
+    def carry_on(hop, downward):
+        slot = home_of(hop, downward) * CORES + core
+
+        @pl.when(received(hop, downward))
+        def _():
+            up_copy(held.at[slot], slot).wait_recv()
+
+        @pl.when(jnp.logical_and(jnp.logical_not(downward), forwards_up(hop)))
+        def _():
+            up_copy(held.at[slot], slot).start()
+
+        @pl.when(jnp.logical_and(downward, forwards_down(hop)))
+        def _():
+            down_copy(held.at[slot], slot).start()
+
+        @pl.when(useful(hop, downward))
+        def _():
+            side_copy(held.at[slot], slot).start()
+
     def substep(index):
+        pl.when(jnp.logical_and(index >= 4, index % 3 != 0))(
+            lambda: carry_on((index - 1) // 3, index % 3 == 2)
+        )
         hop = index // 4
         kind = index % 4
         downward = kind % 2 == 1
         own_core = kind < 2
-        home = home_of(hop, downward)
-        slot = home * CORES + jnp.where(own_core, core, other)
+        slot = home_of(hop, downward) * CORES + jnp.where(own_core, core, other)
         sibling = jnp.logical_and(index == 2, core == 1)
         used = useful(hop, downward)
 
-        @pl.when(jnp.logical_and(own_core, received(hop, downward)))
-        def _():
-            up_copy(held.at[slot], slot).wait_recv()
-
-        @pl.when(jnp.logical_and(kind == 0, forwards_up(hop)))
-        def _():
-            up_copy(held.at[slot], slot).start()
-
-        @pl.when(jnp.logical_and(kind == 1, forwards_down(hop)))
-        def _():
-            down_copy(held.at[slot], slot).start()
-
-        @pl.when(jnp.logical_and(own_core, used))
-        def _():
-            side_copy(held.at[slot], slot).start()
-
         @pl.when(jnp.logical_or(jnp.logical_and(jnp.logical_not(own_core), used), sibling))
         def _():
             side_copy(held.at[slot], slot).wait_recv()
@@ -484,20 +578,37 @@
         def _():
             block_step(slot, held.at[slot], False)
 
-        pl.when(index == GATHER_AT)(gather_stage)
+        pl.when(index == NEAR_AT)(near_stage)
+        pl.when(index == FAR_AT)(far_stage)
         pl.when(index == PARTS_AT)(parts_stage)
         pl.when(index == HIDDEN_AT)(hidden_stage)
         pl.when(index == DOWN_AT)(down_stage)
-
-    loop(max(4 * up_hops + 4, DOWN_AT + 1), substep, 2)
-
-    heads_out[...] = (acc[0:HEAD] / acc[HEAD : HEAD + 1]).astype(jnp.bfloat16)
-    heads_all[tp_me] = heads_out[...]
-    loop(tp_count - 1, lambda turn: head_copy(tp_at(turn), tp_me).start())
+        pl.when(index == RETURN_AT)(return_stage)
+
+    loop(max(4 * up_hops + 4, RETURN_AT + 1), substep, 2)
+
+    heads = acc[0:HEAD] / acc[HEAD : HEAD + 1]
+    heads_all[y_me, x_me] = heads.astype(jnp.bfloat16)
+    loop(wide - 1, lambda turn: row_first(x_at(turn), x_me).start())
+    loop(tall - 1, lambda turn: column_first(y_at(turn), y_me).start())
+    loop(tall - 1, lambda turn: row_part(x_me, y_at(turn)).start())
+    loop(wide - 1, lambda turn: column_part(y_me, x_at(turn)).start())
+
+    def pass_row(turn):
+        row_first(x_at(turn), x_at(turn)).wait_recv()
+        loop(tall - 1, lambda way: row_part(x_at(turn), y_at(way)).start())
+
+    def pass_column(turn):
+        column_first(y_at(turn), y_at(turn)).wait_recv()
+        loop(wide - 1, lambda way: column_part(y_at(turn), x_at(way)).start())
+
+    loop(wide - 1, pass_row)
+    loop(tall - 1, pass_column)
 
     loop(ep_count - 1, lambda turn: result_copy(ep_at(turn), ep_at(turn)).wait_recv())
     own_result().wait()
-    shared_units = hidden_all[:, :, slot_span:].reshape(tp_count * own_hidden, -1)
+    loop(tp_count - 1, lambda turn: shared_copy(tp_at(turn), tp_at(turn)).wait_recv())
+    shared_units = shared_all[...].reshape(tp_count * own_hidden, -1)
     shared_sum = dot(shared_down_ref[...], shared_units).T[0:tokens]
     routed = dot(spread[0], result_in[...]) + dot(spread[1], result_in[...])
     moe_ref[...] = (routed + shared_sum).astype(moe_ref.dtype)
@@ -507,15 +618,21 @@
         result_copy(ep_at(turn), me).wait_send()
 
     loop(ep_count - 1, finish_ep)
-    loop(tall - 1, lambda turn: piece_copy(y_at(turn), y_me).wait_send())
+
+    def finish_pieces(group):
+        loop(tall - 1, lambda turn: piece_copy(group, y_at(turn), y_me).wait_send())
+
+    loop(wide, finish_pieces)
 
     def finish_x(turn):
-        weight_copy(gate_w, 0, x_at(turn), x_me).wait_send()
-        weight_copy(up_w, 1, x_at(turn), x_me).wait_send()
+        for index in range(3):
+            weight_copy(index, x_at(turn), x_me).wait_send()
         part_copy(x_at(turn), x_me).wait_send()
+        cross_copy(x_at(turn), x_me).wait_send()
 
     loop(wide - 1, finish_x)
-    loop(tp_count - 1, lambda turn: hidden_copy(tp_at(turn), tp_me).wait_send())
+    loop(tall - 1, lambda turn: hidden_copy(y_at(turn), y_me).wait_send())
+    loop(tp_count - 1, lambda turn: shared_copy(tp_at(turn), tp_me).wait_send())
 
     @pl.when(chip < chips - 1)
     def _():
@@ -551,13 +668,42 @@
 
     loop(up_hops + 1, finish_hop, 1)
 
-    loop(tp_count - 1, lambda turn: head_copy(tp_at(turn), tp_at(turn)).wait_recv())
+    def wait_far(turn):
+        y = y_at(turn)
+
+        def one(way):
+            x = lax.rem(x_me + way, wide)
+            column_copy(y, x, 0, 0, column_send.at[0, 0, 0]).wait_recv()
+
+        loop(wide, one)
+
+    def wait_wide(turn):
+        x = x_at(turn)
+
+        def one(way):
+            y = lax.rem(y_me + way, tall)
+            row_copy(y, x, 1, 0, row_send.at[0, 0, 0]).wait_recv()
+
+        loop(tall, one)
+
+    loop(tall - 1, wait_far)
+    loop(wide - 1, wait_wide)
     for start in range(0, rows, tile):
         span = slice(start, start + tile)
-        units = heads_all[:, :, span].reshape(tp_count * HEAD, tile)
+        units = heads_all[:, :, :, span].reshape(tp_count * HEAD, tile)
         mixed = dot(out_weight_ref[...], units)
         mixer_ref[span, :] = mixed.T.astype(mixer_ref.dtype)
-    loop(tp_count - 1, lambda turn: head_copy(tp_at(turn), tp_me).wait_send())
+
+    def finish_row(turn):
+        row_first(x_at(turn), x_me).wait_send()
+        loop(tall, lambda y: column_part(y, x_at(turn)).wait_send())
+
+    def finish_column(turn):
+        column_first(y_at(turn), y_me).wait_send()
+        loop(wide, lambda x: row_part(x, y_at(turn)).wait_send())
+
+    loop(wide - 1, finish_row)
+    loop(tall - 1, finish_column)
 
 
 def slot_tables(ep_count, experts, cap, room):
@@ -569,7 +715,8 @@
     places[slot[real], expert[real]] = 1.0
     places[:, LANES] = np.where(real, -(inside % cap), 5.0)
     owner = np.where(real, inside // cap, 0).astype(np.float32)
-    return jnp.asarray(places, jnp.bfloat16), jnp.asarray(np.tile(owner, (8, 1)), jnp.float32)
+    owner = np.tile(owner[:, None], (1, LANES))
+    return jnp.asarray(places, jnp.bfloat16), jnp.asarray(owner, jnp.float32)
 
 
 def local(
@@ -602,8 +749,8 @@
     cap = 2 * token_count * top_count // expert_count
     room = -(-experts * cap // 8) * 8
     slot_count = ep_count * room
-    slot_span = -(-slot_count // LANES) * LANES
-    hidden_span = slot_span + -(-token_count // LANES) * LANES
+    share_rows = slot_count // wide
+    token_span = -(-token_count // LANES) * LANES
     columns = expert_down.shape[2]
 
     moe_rows = moe_input.astype(jnp.float32)
@@ -649,7 +796,7 @@
             jax.ShapeDtypeStruct((rows, columns), bf16),
             jax.ShapeDtypeStruct((token_count, columns), bf16),
         ],
-        in_specs=[vmem] * 8 + [anywhere] * 2 + [vmem] * 5,
+        in_specs=[vmem] * 8 + [anywhere] * 3 + [vmem] * 4,
         out_specs=[vmem, vmem],
         scratch_shapes=[
             pltpu.VMEM((ep_count, rows, LANES), bf16),
@@ -657,23 +804,28 @@
             pltpu.VMEM((8, rows), jnp.float32),
             pltpu.VMEM((slot_count, LANES), bf16),
             pltpu.VMEM((tall, slot_count, LANES), bf16),
-            pltpu.VMEM((wide, 2, experts, own_hidden, model // wide), bf16),
-            pltpu.VMEM((wide, 2 * own_hidden, slot_count), bf16),
-            pltpu.VMEM((wide, 2 * own_hidden, slot_count), bf16),
-            pltpu.VMEM((own_hidden, hidden_span), bf16),
-            pltpu.VMEM((tp_count, own_hidden, hidden_span), bf16),
+            pltpu.VMEM((2, experts, wide, own_hidden, model // wide), bf16),
+            pltpu.VMEM((wide, experts, tp_count * own_hidden, columns), bf16),
+            pltpu.VMEM((slot_count, 2 * wide * own_hidden), bf16),
+            pltpu.VMEM((wide, share_rows, 2 * wide * own_hidden), bf16),
+            pltpu.VMEM((tall, share_rows, wide * own_hidden), bf16),
+            pltpu.VMEM((own_hidden, token_span), bf16),
+            pltpu.VMEM((tp_count, own_hidden, token_span), bf16),
+            pltpu.VMEM((wide, share_rows, columns), bf16),
             pltpu.VMEM((slot_count, columns), bf16),
             pltpu.VMEM((slot_count, columns), bf16),
             pltpu.VMEM((2, token_count, slot_count), bf16),
-            pltpu.VMEM((HEAD, rows), bf16),
-            pltpu.VMEM((tp_count, HEAD, rows), bf16),
+            pltpu.VMEM((tall, wide, HEAD, rows), bf16),
         ]
         + [dma((ep_count,))] * 8
+        + [dma((wide,))] * 2
+        + [dma((tall, wide))] * 2
+        + [dma((3, wide))] * 2
+        + [dma((wide,))] * 2
         + [dma((tall,))] * 2
-        + [dma((2, wide))] * 2
-        + [dma((wide,))] * 2
-        + [dma((tp_count,))] * 4
-        + [dma((4,))],
+        + [dma((tp_count,))] * 2
+        + [dma((2, tall + 1, wide)), dma((2, wide + 1, tall)), dma((2, tp_count))]
+        + [dma((6,))],
         compiler_params=pltpu.CompilerParams(
             collective_id=0, has_side_effects=True, vmem_limit_bytes=56 * 1024 * 1024
         ),
@@ -692,7 +844,7 @@
         owner,
         expert_gate.transpose(0, 2, 1),
         expert_up.transpose(0, 2, 1),
-        expert_down.transpose(0, 2, 1),
+        expert_down,
         shared_gate.T,
         shared_up.T,
         shared_down.T,

time: 151 us -> 123 us (0.81)
  the two profiles are of different devices: /device:TPU:464 before, /device:TPU:1 now
where the time goes in v2:
time: 123 us
  Pallas kernels  110 us (89%)
  local copies, waits for them, and re-layouts  6.14 us (5%)
  other arithmetic  4.67 us (4%)
    pallas_call x1, Pallas kernels, local(): pl.pallas_call(functools.partial(layer_kernel, cap, room), out_shape=[jax...  110 us
    unnamed x33, local copies, waits for them, and re-layouts  5 us

profile of v2, /device:TPU:1, one launch (start us, length us, event | category | flops | bytes accessed | tf_op | source)
XLA Modules:
  0.0 122.9 jit_solution(7001226370105445712)
XLA Ops:
  0.6 0.0 copy-start.8
  0.6 0.0 copy-start.4
  0.6 0.0 copy-start.3
  0.7 0.1 pad.3.clone
  0.7 1.4 %fusion = f32[192]{0:T(256)S(1)} fusion(bf16[192,2048]{1,0:T(8,128)(2,1)} %param.22), kind=kLoop, calls=%fused_computation.2 | loop fusion | flops 1179456 | bytes 787200 | tf_op jit(solution)/shard_map/reduce_sum | solution.py:759
  2.1 0.0 copy-done.8
  2.1 0.1 fusion.4
  2.3 0.8 fusion.3.ranks_ref
  3.1 0.0 copy-done.3
  3.1 0.6 multiply_bitcast_fusion.q_ref
  3.7 0.0 copy-done.4
  3.7 0.3 negate_reduce_fusion
  4.1 0.0 copy-start.10
  4.1 0.0 copy-start.5
  4.1 0.1 maximum_maximum_fusion
  4.2 0.2 copy.45
  4.3 0.0 copy-start.6
  4.4 0.1 convert_element_type.16
  4.4 0.0 copy-start.2
  4.4 0.0 copy-start.1
  4.4 0.8 copy.46
  5.3 0.0 copy-done.10
  5.3 0.9 select_reduce_fusion.weight_ref
  6.1 0.0 copy-done.5
  6.1 0.0 copy-start
  6.2 0.0 copy-start.9
  6.2 0.1 copy.49
  6.3 0.1 copy.50
  6.4 0.1 maximum_dynamic-update-slice_fusion
  6.5 0.0 copy-done.6
  6.6 0.0 copy-done.2
  6.6 0.0 copy-start.7
  6.6 0.8 copy.47
  7.4 0.0 copy-done.1
  7.4 0.8 copy.48
  8.2 0.0 copy-done
  8.3 0.0 copy-done.9
  8.3 1.1 fusion.2.normed_ref
  9.4 0.0 copy-done.7
  9.4 110.4 %layer.1 = (bf16[768,128]{1,0:T(8,128)(2,1)}, bf16[192,128]{1,0:T(8,128)(2,1)}) custom-call(bf16[64,768]{1,0:T(8,128)(2,1)} %multiply_bitcast_fusion.q_ref, bf16[768,128]{1,0:T(8,128)(2,1)} %copy-done.7, bf16[768,128]{1,0:T(8,128)(2,1)} %bitcast.13, bf16[192,2048]{1,0:T(8,128)(2,1)} %fusion.2.normed_ref, bf16[192,128]{1,0:T(8,128)(2,1)} %fusion.3.ranks_ref, ...), custom_call_target="tpu_custom_call" | custom-call | flops 19327352832 | bytes 8388608 | tf_op jit(solution)/shard_map/layer/pallas_call | solution.py:793
  119.8 1.6 %copy.59 = bf16[768,128]{1,0:T(8,128)(2,1)} copy(bf16[768,128]{1,0:T(8,128)(2,1)} %get-tuple-element.9) | data formatting | bytes 393216
  121.4 1.4 %copy.60 = bf16[192,128]{1,0:T(8,128)(2,1)} copy(bf16[192,128]{1,0:T(8,128)(2,1)} %get-tuple-element.10) | data formatting | bytes 98304
  (10 shorter events, 0.1 us)
Async XLA Ops:
  0.6 1.5 %copy-start.8 = (s32[192,3]{0,1:T(4,128)S(1)}, s32[192,3]{0,1:T(4,128)}, u32[]{:S(2)}) copy-start(s32[192,3]{0,1:T(4,128)} %param.24) | copy-start | bytes 6916
  0.6 3.1 %copy-start.4 = (f32[1,24576]{1,0:T(1,128)S(1)}, f32[1,24576]{1,0:T(1,128)}, u32[]{:S(2)}) copy-start(f32[1,24576]{1,0:T(1,128)} %param.20) | copy-start | bytes 294916
  0.6 2.4 %copy-start.3 = (bf16[768,64]{0,1:T(8,128)(2,1)S(1)}, bf16[768,64]{0,1:T(8,128)(2,1)}, u32[]{:S(2)}) copy-start(bf16[768,64]{0,1:T(8,128)(2,1)} %param.17) | copy-start | bytes 294916
  4.1 1.2 copy-start.10
  4.1 2.1 %copy-start.5 = (bf16[768,64]{0,1:T(8,128)(2,1)S(1)}, bf16[768,64]{0,1:T(8,128)(2,1)}, u32[]{:S(2)}) copy-start(bf16[768,64]{0,1:T(8,128)(2,1)} %param.18) | copy-start | bytes 294916
  4.3 2.2 %copy-start.6 = (bf16[768,64]{0,1:T(8,128)(2,1)S(1)}, bf16[768,64]{0,1:T(8,128)(2,1)}, u32[]{:S(2)}) copy-start(bf16[768,64]{0,1:T(8,128)(2,1)} %param.19) | copy-start | bytes 294916
  4.4 2.2 %copy-start.2 = (bf16[512,128]{1,0:T(8,128)(2,1)S(1)}, bf16[512,128]{1,0:T(8,128)(2,1)}, u32[]{:S(2)}) copy-start(bf16[512,128]{1,0:T(8,128)(2,1)} %param.31) | copy-start | bytes 393220
  4.4 3.0 %copy-start.1 = (bf16[1024,128]{1,0:T(8,128)(2,1)S(1)}, bf16[1024,128]{1,0:T(8,128)(2,1)}, u32[]{:S(2)}) copy-start(bf16[1024,128]{1,0:T(8,128)(2,1)} %param.21) | copy-start | bytes 786436
  6.1 2.1 %copy-start = (bf16[192,2048]{1,0:T(8,128)(2,1)S(1)}, bf16[192,2048]{1,0:T(8,128)(2,1)}, u32[]{:S(2)}) copy-start(bf16[192,2048]{1,0:T(8,128)(2,1)} %param.22) | copy-start | bytes 2359300
  6.2 2.1 %copy-start.9 = (f32[2048]{0:T(1024)S(1)}, f32[2048]{0:T(1024)}, u32[]{:S(2)}) copy-start(f32[2048]{0:T(1024)} %param.23) | copy-start | bytes 24580
  6.6 2.8 %copy-start.7 = (bf16[768,128]{1,0:T(8,128)(2,1)}, bf16[768,128]{1,0:T(8,128)(2,1)S(1)}, u32[]{:S(2)}) copy-start(bf16[768,128]{1,0:T(8,128)(2,1)S(1)} %slice_dynamic-update-slice_fusion.kv_ref) | copy-start | bytes 589828

commit v3 on v2

--- a/solution.py
+++ b/solution.py
@@ -17,12 +17,13 @@
 neg_fill = -1e30
 norm_eps = 1e-06
 
+LOCAL_AT = 5
 NEAR_AT = 7
 FAR_AT = 9
 PARTS_AT = 17
-HIDDEN_AT = 24
-DOWN_AT = 27
-RETURN_AT = 31
+HIDDEN_AT = 23
+DOWN_AT = 26
+RETURN_AT = 29
 
 
 def plane_shape(tp_count):
@@ -55,11 +56,13 @@
 def layer_kernel(
     cap,
     room,
-    q_ref,
-    kv_ref,
-    terms_ref,
-    normed_ref,
-    ranks_ref,
+    query_ref,
+    key_ref,
+    value_ref,
+    gate_ref,
+    input_ref,
+    gain_ref,
+    routes_ref,
     weight_ref,
     places_ref,
     owner_ref,
@@ -72,6 +75,14 @@
     out_weight_ref,
     mixer_ref,
     moe_ref,
+    q_ref,
+    kv_ref,
+    terms_ref,
+    normed_ref,
+    weight_rows,
+    rank_rows,
+    mix_weight,
+    shared_weight,
     held,
     acc,
     row_max,
@@ -169,17 +180,55 @@
     def feature_lanes(index):
         return pl.ds(pl.multiple_of(index * features, LANES), features)
 
+    model_rows = input_ref[...].astype(jnp.float32)
+    scale = lax.rsqrt(jnp.mean(model_rows * model_rows, axis=1, keepdims=True) + norm_eps)
+    normed_ref[...] = (model_rows * scale * gain_ref[...]).astype(jnp.bfloat16)
+
+    expert_id = lax.broadcasted_iota(jnp.int32, (LANES, tokens), 0)
+    named = jnp.zeros((LANES, tokens), jnp.float32)
+    weight_of = jnp.zeros((LANES, tokens), jnp.float32)
+    for j in range(routes_ref.shape[0]):
+        match = routes_ref[j : j + 1, :] == expert_id
+        named = jnp.where(match, 1.0, named)
+        weight_of = jnp.where(match, weight_ref[j : j + 1, :], weight_of)
+    before = lax.broadcasted_iota(jnp.int32, (tokens, tokens), 0)
+    after = lax.broadcasted_iota(jnp.int32, (tokens, tokens), 1)
+    earlier = jnp.where(before < after, 1.0, 0.0).astype(jnp.bfloat16)
+    ranks = jnp.where(named > 0.0, dot(named.astype(jnp.bfloat16), earlier), -1.0)
+    rank_rows[...] = ranks
+    weight_rows[...] = weight_of
+
     piece_lanes = pl.ds(pl.multiple_of(x_me * features + y_me * LANES, LANES), LANES)
-    column = lax.broadcasted_iota(jnp.int32, (tokens, LANES), 1)
-    marker = jnp.where(column == 0, 1.0, 0.0).astype(jnp.bfloat16)
-    ranks = jnp.concatenate([ranks_ref[...], marker], axis=1)
+    line = lax.broadcasted_iota(jnp.int32, (LANES, tokens), 0)
+    marker = jnp.where(line == 0, 1.0, 0.0).astype(jnp.bfloat16)
+    marked = jnp.concatenate([ranks.astype(jnp.bfloat16), marker], axis=0)
     own_piece = normed_ref[:, piece_lanes]
     for start in range(0, slot_count, slot_tile):
         span = slice(start, start + slot_tile)
-        match = dot_nt(places_ref[span, :], ranks)
+        match = dot(places_ref[span, :], marked)
         pick = jnp.where(match == 0.0, 1.0, 0.0).astype(jnp.bfloat16)
-        rows_of = dot(pick, own_piece).astype(jnp.bfloat16)
-        picked[span, :] = rows_of
+        picked[span, :] = dot(pick, own_piece).astype(jnp.bfloat16)
+
+    q_ref[...] = (query_ref[...].astype(jnp.float32) * HEAD**-0.5).astype(jnp.bfloat16)
+    lines = jnp.concatenate([key_ref[:, 0:half], key_ref[:, half:rows]], axis=0)
+    kv_ref[0:half, :] = lines.astype(jnp.float32).T.astype(jnp.bfloat16)
+    for i in range(chunks):
+        kv_ref[half + HEAD * i : half + HEAD * (i + 1), :] = value_ref[:, LANES * i : LANES * (i + 1)]
+
+    minus = -gate_ref[...].T
+    high = minus.astype(jnp.bfloat16)
+    rest = minus - high.astype(jnp.float32)
+    middle = rest.astype(jnp.bfloat16)
+    low = (rest - middle.astype(jnp.float32)).astype(jnp.bfloat16)
+    gate_rows = gate_ref.shape[0]
+    lane = lax.broadcasted_iota(jnp.int32, (gate_rows, LANES), 1)
+    shift = lax.broadcasted_iota(jnp.int32, (gate_rows, LANES), 0) - (lane // TERMS) * chunks
+    for i in range(chunks):
+        terms = jnp.zeros((LANES, LANES), jnp.float32)
+        for index, part in enumerate((high, middle, low)):
+            spot = jnp.logical_and(shift == i, lane % TERMS == index)
+            terms = terms + dot(part, jnp.where(spot, 1.0, 0.0).astype(jnp.bfloat16))
+        terms_ref[LANES * i : LANES * (i + 1), :] = terms.astype(jnp.bfloat16)
 
     acc[...] = jnp.zeros_like(acc)
     row_max[...] = jnp.full_like(row_max, neg_fill)
@@ -387,9 +436,9 @@
             [source[half + HEAD * i : half + HEAD * (i + 1), :] for i in range(chunks)], axis=1
         )
         values = jnp.concatenate([values, ones], axis=0)
-        for start in range(0, rows, tile):
-            span = slice(start, start + tile)
-            query = q_ref[:, span]
+
+        def score(start):
+            query = q_ref[:, start : start + tile]
             first = dot(early, jnp.concatenate([query, nothing, chosen], axis=0))
             second = dot(late, jnp.concatenate([nothing, query, chosen], axis=0))
             if masked:
@@ -397,7 +446,10 @@
                 k_pos = lax.broadcasted_iota(jnp.int32, first.shape, 0)
                 first = jnp.where(k_pos <= q_pos, first, neg_fill)
                 second = jnp.where(k_pos + half <= q_pos, second, neg_fill)
-            old_max = row_max[0:1, span]
+            return first, second
+
+        def soften(start, first, second):
+            old_max = row_max[0:1, start : start + tile]
             top = jnp.maximum(
                 jnp.max(first, axis=0, keepdims=True), jnp.max(second, axis=0, keepdims=True)
             )
@@ -409,30 +461,51 @@
                 ],
                 axis=0,
             )
-            keep = jnp.exp2((old_max - new_max) * LOG2E)
+            row_max[0:1, start : start + tile] = new_max
+            return probs, jnp.exp2((old_max - new_max) * LOG2E)
+
+        def collect(start, probs, keep):
+            span = slice(start, start + tile)
             acc[:, span] = acc[:, span] * keep + dot(values, probs)
-            row_max[0:1, span] = new_max
+
+        starts = list(range(0, rows, tile))
+        scores = score(starts[0])
+        waiting = None
+        for index, start in enumerate(starts):
+            upcoming = score(starts[index + 1]) if index + 1 < len(starts) else None
+            ready = soften(start, *scores)
+            if waiting is not None:
+                collect(starts[index - 1], *waiting)
+            waiting, scores = ready, upcoming
+        collect(starts[-1], *waiting)
 
     block_step(me, kv_ref, True)
 
-    high = weight_ref[...].astype(jnp.bfloat16)
-    low = (weight_ref[...] - high.astype(jnp.float32)).astype(jnp.bfloat16)
-    for start in range(0, slot_count, slot_tile):
-        span = slice(start, start + slot_tile)
-        match = dot_nt(ranks, places_ref[span, :])
-        for index, part in enumerate((high, low)):
-            value = dot_nt(part, places_ref[span, 0:LANES])
-            spread[index, :, span] = jnp.where(match == 0.0, value, 0.0).astype(jnp.bfloat16)
-    shared = silu(dot_nt(shared_gate_ref[...], normed_ref[...])) * dot_nt(
-        shared_up_ref[...], normed_ref[...]
-    )
-    shared_out[...] = jnp.zeros_like(shared_out)
-    shared_out[:, 0:tokens] = shared.astype(jnp.bfloat16)
-    shared_all[tp_me] = shared_out[...]
-    loop(tp_count - 1, lambda turn: shared_copy(tp_at(turn), tp_me).start())
-
-    def choose(parts, span):
-        owner = owner_ref[span, 0:1]
+    def local_stage():
+        column = lax.broadcasted_iota(jnp.int32, (tokens, LANES), 1)
+        marker = jnp.where(column == 0, 1.0, 0.0).astype(jnp.bfloat16)
+        marked = jnp.concatenate([rank_rows[...].T.astype(jnp.bfloat16), marker], axis=1)
+        weight = weight_rows[...].T
+        high = weight.astype(jnp.bfloat16)
+        low = (weight - high.astype(jnp.float32)).astype(jnp.bfloat16)
+        for start in range(0, slot_count, slot_tile):
+            span = slice(start, start + slot_tile)
+            match = dot_nt(marked, places_ref[span, :])
+            for index, part in enumerate((high, low)):
+                value = dot_nt(part, places_ref[span, 0:LANES])
+                spread[index, :, span] = jnp.where(match == 0.0, value, 0.0).astype(jnp.bfloat16)
+        shared = silu(dot_nt(shared_gate_ref[...], normed_ref[...])) * dot_nt(
+            shared_up_ref[...], normed_ref[...]
+        )
+        shared_out[...] = jnp.zeros_like(shared_out)
+        shared_out[:, 0:tokens] = shared.astype(jnp.bfloat16)
+        shared_all[tp_me] = shared_out[...]
+        loop(tp_count - 1, lambda turn: shared_copy(tp_at(turn), tp_me).start())
+        mix_weight[...] = out_weight_ref[...].astype(jnp.float32).T.astype(jnp.bfloat16)
+        shared_weight[...] = shared_down_ref[...].astype(jnp.float32).T.astype(jnp.bfloat16)
+
+    def choose(parts):
+        owner = owner_ref[:, 0:1]
         value = parts[0]
         for index in range(1, experts):
             value = jnp.where(owner == float(index), parts[index], value)
@@ -466,8 +539,7 @@
             own_weight(index).wait()
 
         def one_tile(index):
-            start = pl.multiple_of(index * slot_tile, slot_tile)
-            span = pl.ds(start, slot_tile)
+            span = share_of(index)
             rows_of = jnp.concatenate([pieces[y, span, :] for y in range(tall)], axis=1)
             parts = []
             for e in range(experts):
@@ -475,9 +547,9 @@
                     [weights[g, e].reshape(wide * own_hidden, features) for g in range(2)], axis=0
                 )
                 parts.append(dot_nt(rows_of, block))
-            part_out[span, :] = choose(parts, span).astype(jnp.bfloat16)
-
-        loop(slot_count // slot_tile, one_tile)
+            part_out[span, :] = choose(parts).astype(jnp.bfloat16)
+
+        loop(wide, one_tile)
         loop(wide - 1, lambda turn: part_copy(x_at(turn), x_me).start())
 
     def hidden_stage():
@@ -501,7 +573,7 @@
                 dot(units, jnp.concatenate([down_all[x, e], down_all[x + 1, e]], axis=1))
                 for e in range(experts)
             ]
-            result = choose(results, slice(0, share_rows)).astype(jnp.bfloat16)
+            result = choose(results).astype(jnp.bfloat16)
             columns = result.shape[1] // 2
             result_out[x] = result[:, 0:columns]
             result_out[x + 1] = result[:, columns:]
@@ -578,6 +650,7 @@
         def _():
             block_step(slot, held.at[slot], False)
 
+        pl.when(index == LOCAL_AT)(local_stage)
         pl.when(index == NEAR_AT)(near_stage)
         pl.when(index == FAR_AT)(far_stage)
         pl.when(index == PARTS_AT)(parts_stage)
@@ -609,7 +682,7 @@
     own_result().wait()
     loop(tp_count - 1, lambda turn: shared_copy(tp_at(turn), tp_at(turn)).wait_recv())
     shared_units = shared_all[...].reshape(tp_count * own_hidden, -1)
-    shared_sum = dot(shared_down_ref[...], shared_units).T[0:tokens]
+    shared_sum = dot(shared_weight[...], shared_units).T[0:tokens]
     routed = dot(spread[0], result_in[...]) + dot(spread[1], result_in[...])
     moe_ref[...] = (routed + shared_sum).astype(moe_ref.dtype)
 
@@ -691,7 +764,7 @@
     for start in range(0, rows, tile):
         span = slice(start, start + tile)
         units = heads_all[:, :, :, span].reshape(tp_count * HEAD, tile)
-        mixed = dot(out_weight_ref[...], units)
+        mixed = dot(mix_weight[...], units)
         mixer_ref[span, :] = mixed.T.astype(mixer_ref.dtype)
 
     def finish_row(turn):
@@ -706,7 +779,7 @@
     loop(tall - 1, finish_column)
 
 
-def slot_tables(ep_count, experts, cap, room):
+def slot_tables(ep_count, wide, experts, cap, room):
     slot = np.arange(ep_count * room)
     inside = slot % room
     real = inside < experts * cap
@@ -715,7 +788,7 @@
     places[slot[real], expert[real]] = 1.0
     places[:, LANES] = np.where(real, -(inside % cap), 5.0)
     owner = np.where(real, inside // cap, 0).astype(np.float32)
-    owner = np.tile(owner[:, None], (1, LANES))
+    owner = np.tile(owner[: slot.size // wide, None], (1, LANES))
     return jnp.asarray(places, jnp.bfloat16), jnp.asarray(owner, jnp.float32)
 
 
@@ -737,8 +810,6 @@
     shared_down,
 ):
     rows, width = query_rows.shape
-    half = rows // 2
-    chunks = rows // LANES
     token_count = moe_input.shape[0]
     top_count = routes.shape[1]
     experts, model, own_hidden = expert_gate.shape
@@ -753,38 +824,7 @@
     token_span = -(-token_count // LANES) * LANES
     columns = expert_down.shape[2]
 
-    moe_rows = moe_input.astype(jnp.float32)
-    normed = (
-        moe_rows
-        * lax.rsqrt(jnp.mean(moe_rows * moe_rows, axis=1, keepdims=True) + norm_eps)
-        * moe_gain
-    ).astype(jnp.bfloat16)
-    expert_ids = jnp.arange(LANES, dtype=jnp.int32)
-    chosen = routes[:, :, None] == expert_ids[None, None, :]
-    named = jnp.any(chosen, axis=1)
-    weight_of = jnp.sum(jnp.where(chosen, route_weight[:, :, None], 0.0), axis=1)
-    order = jnp.arange(token_count)
-    earlier = (order[None, :] < order[:, None]).astype(jnp.bfloat16)
-    ranks = jnp.dot(earlier, named.astype(jnp.bfloat16), preferred_element_type=jnp.float32)
-    ranks = jnp.where(named, ranks, -1.0).astype(jnp.bfloat16)
-
-    queries = query_rows.T * jnp.asarray(HEAD**-0.5, jnp.bfloat16)
-    value_cols = value_rows.T
-    key_value = jnp.concatenate(
-        [jnp.concatenate([key_rows[:half], key_rows[half:]], axis=1)]
-        + [value_cols[:, LANES * i : LANES * (i + 1)] for i in range(chunks)],
-        axis=0,
-    )
-    minus = -cum_gate.reshape(ep_count, rows)
-    first = lax.reduce_precision(minus, 8, 7)
-    rest = minus - first
-    second = lax.reduce_precision(rest, 8, 7)
-    third = rest - second
-    terms = jnp.stack([first, second, third, jnp.zeros_like(third)], axis=1).astype(jnp.bfloat16)
-    terms = terms.reshape(ep_count * TERMS, rows)
-    terms = jnp.pad(terms, ((0, LANES - ep_count * TERMS), (0, 0))).T
-
-    places, owner = slot_tables(ep_count, experts, cap, room)
+    places, owner = slot_tables(ep_count, wide, experts, cap, room)
     dma = pltpu.SemaphoreType.DMA
     vmem = pl.BlockSpec(memory_space=pltpu.VMEM)
     anywhere = pl.BlockSpec(memory_space=pl.ANY)
@@ -796,9 +836,17 @@
             jax.ShapeDtypeStruct((rows, columns), bf16),
             jax.ShapeDtypeStruct((token_count, columns), bf16),
         ],
-        in_specs=[vmem] * 8 + [anywhere] * 3 + [vmem] * 4,
+        in_specs=[vmem] * 10 + [anywhere] * 3 + [vmem] * 4,
         out_specs=[vmem, vmem],
         scratch_shapes=[
+            pltpu.VMEM((HEAD, rows), bf16),
+            pltpu.VMEM((rows, LANES), bf16),
+            pltpu.VMEM((rows, LANES), bf16),
+            pltpu.VMEM((token_count, model), bf16),
+            pltpu.VMEM((LANES, token_count), jnp.float32),
+            pltpu.VMEM((LANES, token_count), jnp.float32),
+            pltpu.VMEM((columns, tp_count * HEAD), bf16),
+            pltpu.VMEM((columns, tp_count * own_hidden), bf16),
             pltpu.VMEM((ep_count, rows, LANES), bf16),
             pltpu.VMEM((HEAD + 16, rows), jnp.float32),
             pltpu.VMEM((8, rows), jnp.float32),
@@ -834,12 +882,14 @@
         ),
         name="layer",
     )(
-        queries,
-        key_value,
-        terms,
-        normed,
-        ranks,
-        weight_of,
+        query_rows.T,
+        key_rows.T,
+        value_rows.T,
+        cum_gate.reshape(-1, LANES),
+        moe_input,
+        moe_gain.reshape(1, -1),
+        routes.T,
+        route_weight.T,
         places,
         owner,
         expert_gate.transpose(0, 2, 1),
@@ -847,8 +897,8 @@
         expert_down,
         shared_gate.T,
         shared_up.T,
-        shared_down.T,
-        out_weight.T,
+        shared_down,
+        out_weight,
     )
     return mixer_out, moe_out
 

time: 123 us -> 110 us (0.89)
  other arithmetic: 4.67 us -> 0 us
  local copies, waits for them, and re-layouts: 6.14 us -> 2.25 us
  Pallas kernels: 110 us -> 107 us
    pallas_call x1, Pallas kernels: 110 us -> 107 us  [local(): pl.pallas_call(functools.partial(layer_kernel, cap, room), out_shape=[jax...]
    unnamed x33 -> x4, local copies, waits for them, and re-layouts: 5 us -> 2.25 us
    reduce_sum x2 -> x0, other arithmetic: 2.24 us -> none  [the longest x1 1.37 us: local(): jnp.mean(moe_rows * moe_rows, axis=1, keepdims=True) + norm_eps]
where the time goes in v3:
time: 110 us
  Pallas kernels  107 us (97%)
  local copies, waits for them, and re-layouts  2.25 us (2%)
    pallas_call x1, Pallas kernels, local(): pl.pallas_call(functools.partial(layer_kernel, cap, room), out_shape=[jax...  107 us
    unnamed x4, local copies, waits for them, and re-layouts  2.25 us

profile of v3, /device:TPU:1, one launch (start us, length us, event | category | flops | bytes accessed | tf_op | source)
XLA Modules:
  0.0 110.1 jit_solution(236862424145453271)
XLA Ops:
  0.6 107.2 %layer.1 = (bf16[768,128]{1,0:T(8,128)(2,1)}, bf16[192,128]{1,0:T(8,128)(2,1)}) custom-call(bf16[64,768]{1,0:T(8,128)(2,1)} %bitcast.15, bf16[64,768]{1,0:T(8,128)(2,1)} %bitcast.16, bf16[64,768]{1,0:T(8,128)(2,1)} %bitcast.17, f32[192,128]{1,0:T(8,128)} %bitcast.18, bf16[192,2048]{1,0:T(8,128)(2,1)} %input_ref.1, f32[1,2048]{1,0:T(1,128)} %bitcast.19, ...), custom_call_target="tpu_custom_call" | custom-call | flops 19327352832 | bytes 8388608 | tf_op jit(solution)/shard_map/layer/pallas_call | solution.py:833
  107.8 0.0 copy-start
  107.8 1.6 %copy.21 = bf16[768,128]{1,0:T(8,128)(2,1)} copy(bf16[768,128]{1,0:T(8,128)(2,1)} %get-tuple-element.4) | data formatting | bytes 393216
  109.5 0.0 copy-done
  109.5 0.6 copy.22
Async XLA Ops:
  107.8 1.6 %copy-start = (bf16[192,128]{1,0:T(8,128)(2,1)S(1)}, bf16[192,128]{1,0:T(8,128)(2,1)}, u32[]{:S(2)}) copy-start(bf16[192,128]{1,0:T(8,128)(2,1)} %get-tuple-element.5) | copy-start | bytes 147460

commit v4 on v3

--- a/solution.py
+++ b/solution.py
@@ -18,12 +18,11 @@
 norm_eps = 1e-06
 
 LOCAL_AT = 5
-NEAR_AT = 7
-FAR_AT = 9
-PARTS_AT = 17
-HIDDEN_AT = 23
-DOWN_AT = 26
-RETURN_AT = 29
+GATHER_AT = (7, 10)
+PARTS_AT = (9, 16)
+HIDDEN_AT = (12, 20)
+DOWN_AT = (19, 24)
+RETURN_AT = (23, 28)
 
 
 def plane_shape(tp_count):
@@ -124,6 +123,7 @@
     column_send,
     head_recv,
     own_sem,
+    own_cross_sem,
 ):
     rows = q_ref.shape[1]
     half = rows // 2
@@ -152,7 +152,23 @@
     features = normed_ref.shape[1] // wide
     share = ep_count // wide
     share_rows = share * room
-    keeper = me // share
+    half_share = share // 2
+    half_rows = half_share * room
+    reach = chips // 4
+
+    def place_of(block, home):
+        offset = lax.rem(block // CORES - home // CORES + reach + chips, chips)
+        rank = lax.rem(offset, chips // 2) * CORES + block % CORES
+        far = offset // (chips // 2)
+        return rank // half_share * share + far * half_share + lax.rem(rank, half_share)
+
+    def block_at(rank, far):
+        offset = rank // CORES + far * (chips // 2)
+        return lax.rem(chip - reach + offset + chips, chips) * CORES + rank % CORES
+
+    def target_at(rank, far):
+        offset = rank // CORES + far * (chips // 2)
+        return lax.rem(chip + reach - offset + chips, chips) * CORES + rank % CORES
 
     def ep_at(turn):
         return lax.rem(me + turn + 1, ep_count)
@@ -238,87 +254,83 @@
     def pick_copy(target, owner):
         return pltpu.make_async_remote_copy(
             src_ref=picked.at[room_of(target)],
-            dst_ref=pieces.at[y_me, room_of(owner)],
+            dst_ref=pieces.at[y_me, room_of(place_of(owner, target))],
             send_sem=pick_send.at[target],
             recv_sem=pick_recv.at[owner],
             device_id={"ep": target},
         )
 
-    sources = (
-        (gate_w.at[:, :, feature_lanes(x_me)], lambda owner: weights.at[0, :, owner]),
-        (up_w.at[:, :, feature_lanes(x_me)], lambda owner: weights.at[1, :, owner]),
-        (down_w, lambda owner: down_all.at[owner]),
-    )
-
-    def weight_copy(index, target, owner):
-        source = down_w
+    def weight_ends(index, target, owner):
         if index < 2:
             source = (gate_w, up_w)[index].at[:, :, feature_lanes(target)]
+            return source, weights.at[index, :, owner]
+        return down_w.at[index - 2], down_all.at[owner, index - 2]
+
+    def weight_copy(index, target, owner):
+        source, place = weight_ends(index, target, owner)
         return pltpu.make_async_remote_copy(
             src_ref=source,
-            dst_ref=sources[index][1](owner),
+            dst_ref=place,
             send_sem=weight_send.at[index, target],
             recv_sem=weight_recv.at[index, owner],
             device_id={"tp": y_me * wide + target},
         )
 
     def own_weight(index):
-        return pltpu.make_async_copy(
-            sources[index][0], sources[index][1](x_me), own_sem.at[index]
-        )
-
-    def up_copy(src, slot):
+        source, place = weight_ends(index, x_me, x_me)
+        return pltpu.make_async_copy(source, place, own_sem.at[index])
+
+    weight_count = 2 + experts
+    early_weights = 2 + experts // 2
+
+    def send_weight(index):
+        loop(wide - 1, lambda turn: weight_copy(index, x_at(turn), x_me).start())
+
+    def kv_copy(part, slot, own, send_sem, place):
+        span = pl.ds(part * half, half)
         return pltpu.make_async_remote_copy(
-            src_ref=src,
-            dst_ref=held.at[slot],
-            send_sem=up_send.at[slot],
-            recv_sem=kv_recv.at[slot],
-            device_id={"ep": me + CORES},
-        )
-
-    def down_copy(src, slot):
-        return pltpu.make_async_remote_copy(
-            src_ref=src,
-            dst_ref=held.at[slot],
-            send_sem=down_send.at[slot],
-            recv_sem=kv_recv.at[slot],
-            device_id={"ep": lax.rem(chip + chips - 1, chips) * CORES + core},
-        )
-
-    def side_copy(src, slot):
-        return pltpu.make_async_remote_copy(
-            src_ref=src,
-            dst_ref=held.at[slot],
-            send_sem=side_send.at[slot],
-            recv_sem=kv_recv.at[slot],
-            device_id={"ep": chip * CORES + other},
-        )
-
-    def piece_copy(group, target, owner):
-        place = pieces.at[owner, pl.ds(pl.multiple_of(group * share_rows, 8), share_rows)]
+            src_ref=kv_ref.at[span] if own else held.at[slot, span],
+            dst_ref=held.at[slot, span],
+            send_sem=send_sem.at[part, slot],
+            recv_sem=kv_recv.at[part, slot],
+            device_id={"ep": place},
+        )
+
+    def up_copy(part, slot, own=False):
+        return kv_copy(part, slot, own, up_send, me + CORES)
+
+    def down_copy(part, slot, own=False):
+        below = lax.rem(chip + chips - 1, chips) * CORES + core
+        return kv_copy(part, slot, own, down_send, below)
+
+    def side_copy(part, slot, own=False):
+        return kv_copy(part, slot, own, side_send, chip * CORES + other)
+
+    def piece_copy(far, group, target, owner):
+        place = pieces.at[owner, rows_at(group, far)]
         return pltpu.make_async_remote_copy(
             src_ref=place,
             dst_ref=place,
-            send_sem=piece_send.at[target, group],
-            recv_sem=piece_recv.at[owner, group],
+            send_sem=piece_send.at[target, far * wide + group],
+            recv_sem=piece_recv.at[owner, far * wide + group],
             device_id={"tp": target * wide + x_me},
         )
 
-    def part_copy(target, owner):
+    def part_copy(far, target, owner):
         return pltpu.make_async_remote_copy(
-            src_ref=part_out.at[pl.ds(pl.multiple_of(target * share_rows, 8), share_rows)],
-            dst_ref=part_in.at[owner],
-            send_sem=part_send.at[target],
-            recv_sem=part_recv.at[owner],
+            src_ref=part_out.at[rows_at(target, far)],
+            dst_ref=part_in.at[owner, far],
+            send_sem=part_send.at[far, target],
+            recv_sem=part_recv.at[far, owner],
             device_id={"tp": y_me * wide + target},
         )
 
-    def hidden_copy(target, owner):
+    def hidden_copy(far, target, owner):
         return pltpu.make_async_remote_copy(
-            src_ref=hidden_all.at[owner],
-            dst_ref=hidden_all.at[owner],
-            send_sem=hidden_send.at[target],
-            recv_sem=hidden_recv.at[owner],
+            src_ref=hidden_all.at[owner, far],
+            dst_ref=hidden_all.at[owner, far],
+            send_sem=hidden_send.at[far, target],
+            recv_sem=hidden_recv.at[far, owner],
             device_id={"tp": target * wide + x_me},
         )
 
@@ -331,26 +343,27 @@
             device_id={"tp": target},
         )
 
-    def share_of(index):
-        return pl.ds(pl.multiple_of(index * share_rows, 8), share_rows)
-
-    def cross_copy(target, owner):
+    def rows_at(index, far):
+        start = index * share_rows + far * half_rows
+        return pl.ds(pl.multiple_of(start, 8), half_rows)
+
+    def cross_copy(far, target, owner):
         return pltpu.make_async_remote_copy(
-            src_ref=result_out.at[target],
-            dst_ref=result_all.at[share_of(owner)],
-            send_sem=cross_send.at[target],
-            recv_sem=cross_recv.at[owner],
+            src_ref=result_out.at[target, far],
+            dst_ref=result_all.at[rows_at(owner, far)],
+            send_sem=cross_send.at[far, target],
+            recv_sem=cross_recv.at[far, owner],
             device_id={"tp": y_me * wide + target},
         )
 
-    def own_cross():
+    def own_cross(far):
         return pltpu.make_async_copy(
-            result_out.at[x_me], result_all.at[share_of(x_me)], own_sem.at[5]
+            result_out.at[x_me, far], result_all.at[rows_at(x_me, far)], own_cross_sem.at[far]
         )
 
     def result_copy(target, owner):
         return pltpu.make_async_remote_copy(
-            src_ref=result_all.at[room_of(target)],
+            src_ref=result_all.at[room_of(place_of(target, me))],
             dst_ref=result_in.at[room_of(owner)],
             send_sem=result_send.at[target],
             recv_sem=result_recv.at[owner],
@@ -359,7 +372,9 @@
 
     def own_result():
         return pltpu.make_async_copy(
-            result_all.at[room_of(me)], result_in.at[room_of(me)], own_sem.at[4]
+            result_all.at[room_of(place_of(me, me))],
+            result_in.at[room_of(me)],
+            own_sem.at[weight_count],
         )
 
     half_head = HEAD // 2
@@ -398,29 +413,42 @@
 
     def own_pick():
         return pltpu.make_async_copy(
-            picked.at[room_of(me)], pieces.at[y_me, room_of(me)], own_sem.at[3]
+            picked.at[room_of(me)],
+            pieces.at[y_me, room_of(place_of(me, me))],
+            own_sem.at[weight_count + 1],
         )
 
     @pl.when(chip < chips - 1)
     def _():
-        up_copy(kv_ref, me).start()
+        for part in range(2):
+            up_copy(part, me, True).start()
 
     @pl.when(chip <= last_down)
     def _():
-        down_copy(kv_ref, me).start()
+        for part in range(2):
+            down_copy(part, me, True).start()
 
     @pl.when(core == 0)
     def _():
-        side_copy(kv_ref, me).start()
-
-    loop(ep_count - 1, lambda turn: pick_copy(ep_at(turn), me).start())
+        for part in range(2):
+            side_copy(part, me, True).start()
+
+    def send_picked(far):
+        def one(rank):
+            target = target_at(rank, far)
+
+            @pl.when(target != me)
+            def _():
+                pick_copy(target, me).start()
+
+        loop(ep_count // 2, one)
+
+    send_picked(0)
     own_pick().start()
-
-    loop(wide - 1, lambda turn: weight_copy(0, x_at(turn), x_me).start())
-    loop(wide - 1, lambda turn: weight_copy(1, x_at(turn), x_me).start())
-    for index in range(3):
+    for index in range(weight_count):
         own_weight(index).start()
-    loop(wide - 1, lambda turn: weight_copy(2, x_at(turn), x_me).start())
+    for index in range(early_weights):
+        send_weight(index)
 
     ones = jnp.ones((acc.shape[0] - HEAD, rows), jnp.bfloat16)
     nothing = jnp.zeros((HEAD, tile), jnp.bfloat16)
@@ -482,6 +510,8 @@
     block_step(me, kv_ref, True)
 
     def local_stage():
+        send_picked(1)
+
         column = lax.broadcasted_iota(jnp.int32, (tokens, LANES), 1)
         marker = jnp.where(column == 0, 1.0, 0.0).astype(jnp.bfloat16)
         marked = jnp.concatenate([rank_rows[...].T.astype(jnp.bfloat16), marker], axis=1)
@@ -505,69 +535,87 @@
         shared_weight[...] = shared_down_ref[...].astype(jnp.float32).T.astype(jnp.bfloat16)
 
     def choose(parts):
-        owner = owner_ref[:, 0:1]
+        owner = owner_ref[0 : parts[0].shape[0], 0:1]
         value = parts[0]
         for index in range(1, experts):
             value = jnp.where(owner == float(index), parts[index], value)
         return value
 
-    def forward_group(group):
-        def wait_block(turn):
-            source = group * share + turn
-
-            @pl.when(source != me)
-            def _():
-                pick_copy(source, source).wait_recv()
-
-        loop(share, wait_block)
-        loop(tall - 1, lambda turn: piece_copy(group, y_at(turn), y_me).start())
-
-    def near_stage():
-        own_pick().wait()
-        forward_group(keeper)
-
-    def far_stage():
-        loop(wide, lambda turn: forward_group(lax.rem(keeper + turn, wide)), 1)
-
-    def parts_stage():
+    def gather_stage(far):
+        @pl.when(far == 0)
+        def _():
+            own_pick().wait()
+
+        def one_group(group):
+            def wait_block(turn):
+                source = block_at(group * half_share + turn, far)
+
+                @pl.when(source != me)
+                def _():
+                    pick_copy(source, source).wait_recv()
+
+            loop(half_share, wait_block)
+            loop(tall - 1, lambda turn: piece_copy(far, group, y_at(turn), y_me).start())
+
+        loop(wide, one_group)
+
+    def parts_stage(far):
         def wait_pieces(group):
-            loop(tall - 1, lambda turn: piece_copy(group, y_at(turn), y_at(turn)).wait_recv())
+            loop(tall - 1, lambda turn: piece_copy(far, group, y_at(turn), y_at(turn)).wait_recv())
 
         loop(wide, wait_pieces)
-        for index in range(2):
-            loop(wide - 1, lambda turn: weight_copy(index, x_at(turn), x_at(turn)).wait_recv())
-            own_weight(index).wait()
-
-        def one_tile(index):
-            span = share_of(index)
-            rows_of = jnp.concatenate([pieces[y, span, :] for y in range(tall)], axis=1)
-            parts = []
-            for e in range(experts):
-                block = jnp.concatenate(
-                    [weights[g, e].reshape(wide * own_hidden, features) for g in range(2)], axis=0
-                )
-                parts.append(dot_nt(rows_of, block))
-            part_out[span, :] = choose(parts).astype(jnp.bfloat16)
-
-        loop(wide, one_tile)
-        loop(wide - 1, lambda turn: part_copy(x_at(turn), x_me).start())
-
-    def hidden_stage():
-        loop(wide - 1, lambda turn: part_copy(x_at(turn), x_at(turn)).wait_recv())
-        own_rows = pl.ds(pl.multiple_of(x_me * share_rows, 8), share_rows)
-        total = part_out[own_rows, :].astype(jnp.float32)
+
+        @pl.when(far == 0)
+        def _():
+            for index in range(2):
+                loop(wide - 1, lambda turn: weight_copy(index, x_at(turn), x_at(turn)).wait_recv())
+                own_weight(index).wait()
+
+        rows_of = jnp.concatenate(
+            [
+                jnp.concatenate([pieces[y, rows_at(group, far), :] for group in range(wide)], axis=0)
+                for y in range(tall)
+            ],
+            axis=1,
+        )
+        parts = []
+        for e in range(experts):
+            block = jnp.concatenate(
+                [weights[g, e].reshape(wide * own_hidden, features) for g in range(2)], axis=0
+            )
+            parts.append(dot_nt(rows_of, block))
+        chosen_parts = choose(parts).astype(jnp.bfloat16)
+        for group in range(wide):
+            part_out[rows_at(group, far), :] = chosen_parts[
+                group * half_rows : (group + 1) * half_rows
+            ]
+        loop(wide - 1, lambda turn: part_copy(far, x_at(turn), x_me).start())
+
+        @pl.when(far == 0)
+        def _():
+            for index in range(early_weights, weight_count):
+                send_weight(index)
+
+    def hidden_stage(far):
+        loop(wide - 1, lambda turn: part_copy(far, x_at(turn), x_at(turn)).wait_recv())
+        total = part_out[rows_at(x_me, far), :].astype(jnp.float32)
         for turn in range(wide - 1):
-            total = total + part_in[x_at(turn)].astype(jnp.float32)
+            total = total + part_in[x_at(turn), far].astype(jnp.float32)
         middle = wide * own_hidden
         hidden = silu(total[:, 0:middle]) * total[:, middle:]
-        hidden_all[y_me] = hidden.astype(jnp.bfloat16)
-        loop(tall - 1, lambda turn: hidden_copy(y_at(turn), y_me).start())
-
-    def down_stage():
-        loop(tall - 1, lambda turn: hidden_copy(y_at(turn), y_at(turn)).wait_recv())
-        loop(wide - 1, lambda turn: weight_copy(2, x_at(turn), x_at(turn)).wait_recv())
-        own_weight(2).wait()
-        units = jnp.concatenate([hidden_all[y] for y in range(tall)], axis=1)
+        hidden_all[y_me, far] = hidden.astype(jnp.bfloat16)
+        loop(tall - 1, lambda turn: hidden_copy(far, y_at(turn), y_me).start())
+
+    def down_stage(far):
+        loop(tall - 1, lambda turn: hidden_copy(far, y_at(turn), y_at(turn)).wait_recv())
+
+        @pl.when(far == 0)
+        def _():
+            for index in range(2, weight_count):
+                loop(wide - 1, lambda turn: weight_copy(index, x_at(turn), x_at(turn)).wait_recv())
+                own_weight(index).wait()
+
+        units = jnp.concatenate([hidden_all[y, far] for y in range(tall)], axis=1)
         for x in range(0, wide, 2):
             results = [
                 dot(units, jnp.concatenate([down_all[x, e], down_all[x + 1, e]], axis=1))
@@ -575,17 +623,27 @@
             ]
             result = choose(results).astype(jnp.bfloat16)
             columns = result.shape[1] // 2
-            result_out[x] = result[:, 0:columns]
-            result_out[x + 1] = result[:, columns:]
-
-        loop(wide - 1, lambda turn: cross_copy(x_at(turn), x_me).start())
-        own_cross().start()
-
-    def return_stage():
-        loop(wide - 1, lambda turn: cross_copy(x_at(turn), x_at(turn)).wait_recv())
-        own_cross().wait()
-        loop(ep_count - 1, lambda turn: result_copy(ep_at(turn), me).start())
-        own_result().start()
+            result_out[x, far] = result[:, 0:columns]
+            result_out[x + 1, far] = result[:, columns:]
+        loop(wide - 1, lambda turn: cross_copy(far, x_at(turn), x_me).start())
+        own_cross(far).start()
+
+    def return_stage(far):
+        loop(wide - 1, lambda turn: cross_copy(far, x_at(turn), x_at(turn)).wait_recv())
+        own_cross(far).wait()
+
+        def one(rank):
+            target = block_at(rank, far)
+
+            @pl.when(target != me)
+            def _():
+                result_copy(target, me).start()
+
+        loop(ep_count // 2, one)
+
+        @pl.when(far == 0)
+        def _():
+            own_result().start()
 
     def received(hop, downward):
         going_up = jnp.logical_and(hop >= 1, jnp.logical_and(hop <= up_hops, chip - hop >= 0))
@@ -597,7 +655,7 @@
 
     def useful(hop, downward):
         return jnp.logical_and(
-            received(hop, downward), jnp.logical_or(jnp.logical_not(downward), chip + hop >= chips)
+            received(hop, downward), jnp.where(downward, chip + hop >= chips, True)
         )
 
     def forwards_up(hop):
@@ -611,29 +669,43 @@
     def home_of(hop, downward):
         return jnp.where(downward, lax.rem(chip + hop, chips), chip - hop)
 
-    def carry_on(hop, downward):
+    def carry_on(part, hop, downward):
         slot = home_of(hop, downward) * CORES + core
 
         @pl.when(received(hop, downward))
         def _():
-            up_copy(held.at[slot], slot).wait_recv()
-
-        @pl.when(jnp.logical_and(jnp.logical_not(downward), forwards_up(hop)))
-        def _():
-            up_copy(held.at[slot], slot).start()
-
-        @pl.when(jnp.logical_and(downward, forwards_down(hop)))
-        def _():
-            down_copy(held.at[slot], slot).start()
+            up_copy(part, slot).wait_recv()
+
+        if downward:
+
+            @pl.when(forwards_down(hop))
+            def _():
+                down_copy(part, slot).start()
+
+        else:
+
+            @pl.when(forwards_up(hop))
+            def _():
+                up_copy(part, slot).start()
 
         @pl.when(useful(hop, downward))
         def _():
-            side_copy(held.at[slot], slot).start()
+            side_copy(part, slot).start()
 
     def substep(index):
-        pl.when(jnp.logical_and(index >= 4, index % 3 != 0))(
-            lambda: carry_on((index - 1) // 3, index % 3 == 2)
-        )
+        @pl.when(jnp.logical_and(index >= 3, index % 3 == 0))
+        def _():
+            carry_on(0, index // 3, False)
+
+        @pl.when(jnp.logical_and(index >= 3, index % 3 == 1))
+        def _():
+            carry_on(1, index // 3, False)
+            carry_on(0, index // 3, True)
+
+        @pl.when(jnp.logical_and(index >= 3, index % 3 == 2))
+        def _():
+            carry_on(1, index // 3, True)
+
         hop = index // 4
         kind = index % 4
         downward = kind % 2 == 1
@@ -644,21 +716,28 @@
 
         @pl.when(jnp.logical_or(jnp.logical_and(jnp.logical_not(own_core), used), sibling))
         def _():
-            side_copy(held.at[slot], slot).wait_recv()
+            for part in range(2):
+                side_copy(part, slot).wait_recv()
 
         @pl.when(jnp.logical_or(used, sibling))
         def _():
             block_step(slot, held.at[slot], False)
 
         pl.when(index == LOCAL_AT)(local_stage)
-        pl.when(index == NEAR_AT)(near_stage)
-        pl.when(index == FAR_AT)(far_stage)
-        pl.when(index == PARTS_AT)(parts_stage)
-        pl.when(index == HIDDEN_AT)(hidden_stage)
-        pl.when(index == DOWN_AT)(down_stage)
-        pl.when(index == RETURN_AT)(return_stage)
-
-    loop(max(4 * up_hops + 4, RETURN_AT + 1), substep, 2)
+        for stage, times in (
+            (gather_stage, GATHER_AT),
+            (parts_stage, PARTS_AT),
+            (hidden_stage, HIDDEN_AT),
+            (down_stage, DOWN_AT),
+            (return_stage, RETURN_AT),
+        ):
+            far = jnp.where(index == times[1], 1, 0)
+
+            @pl.when(jnp.logical_or(index == times[0], index == times[1]))
+            def _():
+                stage(far)
+
+    loop(max(4 * up_hops + 4, RETURN_AT[1] + 1), substep, 2)
 
     heads = acc[0:HEAD] / acc[HEAD : HEAD + 1]
     heads_all[y_me, x_me] = heads.astype(jnp.bfloat16)
@@ -692,52 +771,60 @@
 
     loop(ep_count - 1, finish_ep)
 
-    def finish_pieces(group):
-        loop(tall - 1, lambda turn: piece_copy(group, y_at(turn), y_me).wait_send())
-
-    loop(wide, finish_pieces)
-
-    def finish_x(turn):
-        for index in range(3):
-            weight_copy(index, x_at(turn), x_me).wait_send()
-        part_copy(x_at(turn), x_me).wait_send()
-        cross_copy(x_at(turn), x_me).wait_send()
-
-    loop(wide - 1, finish_x)
-    loop(tall - 1, lambda turn: hidden_copy(y_at(turn), y_me).wait_send())
+    def finish_half(far):
+        def finish_pieces(group):
+            loop(tall - 1, lambda turn: piece_copy(far, group, y_at(turn), y_me).wait_send())
+
+        loop(wide, finish_pieces)
+
+        def finish_x(turn):
+            part_copy(far, x_at(turn), x_me).wait_send()
+            cross_copy(far, x_at(turn), x_me).wait_send()
+
+        loop(wide - 1, finish_x)
+        loop(tall - 1, lambda turn: hidden_copy(far, y_at(turn), y_me).wait_send())
+
+    loop(2, finish_half)
+    for index in range(weight_count):
+        loop(wide - 1, lambda turn: weight_copy(index, x_at(turn), x_me).wait_send())
     loop(tp_count - 1, lambda turn: shared_copy(tp_at(turn), tp_me).wait_send())
 
     @pl.when(chip < chips - 1)
     def _():
-        up_copy(kv_ref, me).wait_send()
+        for part in range(2):
+            up_copy(part, me, True).wait_send()
 
     @pl.when(chip <= last_down)
     def _():
-        down_copy(kv_ref, me).wait_send()
+        for part in range(2):
+            down_copy(part, me, True).wait_send()
 
     @pl.when(core == 0)
     def _():
-        side_copy(kv_ref, me).wait_send()
+        for part in range(2):
+            side_copy(part, me, True).wait_send()
 
     def finish_hop(hop):
         low_slot = home_of(hop, False) * CORES + core
         high_slot = home_of(hop, True) * CORES + core
 
-        @pl.when(forwards_up(hop))
-        def _():
-            up_copy(held.at[low_slot], low_slot).wait_send()
-
-        @pl.when(forwards_down(hop))
-        def _():
-            down_copy(held.at[high_slot], high_slot).wait_send()
-
-        @pl.when(useful(hop, False))
-        def _():
-            side_copy(held.at[low_slot], low_slot).wait_send()
-
-        @pl.when(useful(hop, True))
-        def _():
-            side_copy(held.at[high_slot], high_slot).wait_send()
+        for part in range(2):
+
+            @pl.when(forwards_up(hop))
+            def _():
+                up_copy(part, low_slot).wait_send()
+
+            @pl.when(forwards_down(hop))
+            def _():
+                down_copy(part, high_slot).wait_send()
+
+            @pl.when(useful(hop, False))
+            def _():
+                side_copy(part, low_slot).wait_send()
+
+            @pl.when(useful(hop, True))
+            def _():
+                side_copy(part, high_slot).wait_send()
 
     loop(up_hops + 1, finish_hop, 1)
 
@@ -779,7 +866,7 @@
     loop(tall - 1, finish_column)
 
 
-def slot_tables(ep_count, wide, experts, cap, room):
+def slot_tables(ep_count, experts, cap, room):
     slot = np.arange(ep_count * room)
     inside = slot % room
     real = inside < experts * cap
@@ -788,7 +875,7 @@
     places[slot[real], expert[real]] = 1.0
     places[:, LANES] = np.where(real, -(inside % cap), 5.0)
     owner = np.where(real, inside // cap, 0).astype(np.float32)
-    owner = np.tile(owner[: slot.size // wide, None], (1, LANES))
+    owner = np.tile(owner[: slot.size // 2, None], (1, LANES))
     return jnp.asarray(places, jnp.bfloat16), jnp.asarray(owner, jnp.float32)
 
 
@@ -824,7 +911,7 @@
     token_span = -(-token_count // LANES) * LANES
     columns = expert_down.shape[2]
 
-    places, owner = slot_tables(ep_count, wide, experts, cap, room)
+    places, owner = slot_tables(ep_count, experts, cap, room)
     dma = pltpu.SemaphoreType.DMA
     vmem = pl.BlockSpec(memory_space=pltpu.VMEM)
     anywhere = pl.BlockSpec(memory_space=pl.ANY)
@@ -855,25 +942,26 @@
             pltpu.VMEM((2, experts, wide, own_hidden, model // wide), bf16),
             pltpu.VMEM((wide, experts, tp_count * own_hidden, columns), bf16),
             pltpu.VMEM((slot_count, 2 * wide * own_hidden), bf16),
-            pltpu.VMEM((wide, share_rows, 2 * wide * own_hidden), bf16),
-            pltpu.VMEM((tall, share_rows, wide * own_hidden), bf16),
+            pltpu.VMEM((wide, 2, share_rows // 2, 2 * wide * own_hidden), bf16),
+            pltpu.VMEM((tall, 2, share_rows // 2, wide * own_hidden), bf16),
             pltpu.VMEM((own_hidden, token_span), bf16),
             pltpu.VMEM((tp_count, own_hidden, token_span), bf16),
-            pltpu.VMEM((wide, share_rows, columns), bf16),
+            pltpu.VMEM((wide, 2, share_rows // 2, columns), bf16),
             pltpu.VMEM((slot_count, columns), bf16),
             pltpu.VMEM((slot_count, columns), bf16),
             pltpu.VMEM((2, token_count, slot_count), bf16),
             pltpu.VMEM((tall, wide, HEAD, rows), bf16),
         ]
-        + [dma((ep_count,))] * 8
-        + [dma((wide,))] * 2
-        + [dma((tall, wide))] * 2
-        + [dma((3, wide))] * 2
-        + [dma((wide,))] * 2
-        + [dma((tall,))] * 2
+        + [dma((2, ep_count))] * 4
+        + [dma((ep_count,))] * 4
+        + [dma((2, wide))] * 2
+        + [dma((tall, 2 * wide))] * 2
+        + [dma((2 + experts, wide))] * 2
+        + [dma((2, wide))] * 2
+        + [dma((2, tall))] * 2
         + [dma((tp_count,))] * 2
         + [dma((2, tall + 1, wide)), dma((2, wide + 1, tall)), dma((2, tp_count))]
-        + [dma((6,))],
+        + [dma((experts + 4,)), dma((2,))],
         compiler_params=pltpu.CompilerParams(
             collective_id=0, has_side_effects=True, vmem_limit_bytes=56 * 1024 * 1024
         ),

time: 110 us -> 105 us (0.955)
  Pallas kernels: 107 us -> 102 us
    pallas_call x1, Pallas kernels: 107 us -> 102 us  [local(): pl.pallas_call(functools.partial(layer_kernel, cap, room), out_shape=[jax...]
where the time goes in v4:
time: 105 us
  Pallas kernels  102 us (97%)
  local copies, waits for them, and re-layouts  2.25 us (2%)
    pallas_call x1, Pallas kernels, local(): pl.pallas_call(functools.partial(layer_kernel, cap, room), out_shape=[jax...  102 us
    unnamed x4, local copies, waits for them, and re-layouts  2.25 us

profile of v4, /device:TPU:1, one launch (start us, length us, event | category | flops | bytes accessed | tf_op | source)
XLA Modules:
  0.0 104.5 jit_solution(3862809476979679088)
XLA Ops:
  0.6 101.6 %layer.1 = (bf16[768,128]{1,0:T(8,128)(2,1)}, bf16[192,128]{1,0:T(8,128)(2,1)}) custom-call(bf16[64,768]{1,0:T(8,128)(2,1)} %bitcast.15, bf16[64,768]{1,0:T(8,128)(2,1)} %bitcast.16, bf16[64,768]{1,0:T(8,128)(2,1)} %bitcast.17, f32[192,128]{1,0:T(8,128)} %bitcast.18, bf16[192,2048]{1,0:T(8,128)(2,1)} %input_ref.1, f32[1,2048]{1,0:T(1,128)} %bitcast.19, ...), custom_call_target="tpu_custom_call" | custom-call | flops 19327352832 | bytes 8388608 | tf_op jit(solution)/shard_map/layer/pallas_call | solution.py:920
  102.3 0.0 copy-start
  102.3 1.6 %copy.21 = bf16[768,128]{1,0:T(8,128)(2,1)} copy(bf16[768,128]{1,0:T(8,128)(2,1)} %get-tuple-element.4) | data formatting | bytes 393216
  103.9 0.0 copy-done
  103.9 0.6 copy.22
Async XLA Ops:
  102.3 1.6 %copy-start = (bf16[192,128]{1,0:T(8,128)(2,1)S(1)}, bf16[192,128]{1,0:T(8,128)(2,1)}, u32[]{:S(2)}) copy-start(bf16[192,128]{1,0:T(8,128)(2,1)} %get-tuple-element.5) | copy-start | bytes 147460

commit v5 on v4

--- a/solution.py
+++ b/solution.py
@@ -754,20 +754,8 @@
         column_first(y_at(turn), y_at(turn)).wait_recv()
         loop(wide - 1, lambda way: column_part(y_at(turn), x_at(way)).start())
 
-    loop(wide - 1, pass_row)
-    loop(tall - 1, pass_column)
-
-    loop(ep_count - 1, lambda turn: result_copy(ep_at(turn), ep_at(turn)).wait_recv())
-    own_result().wait()
-    loop(tp_count - 1, lambda turn: shared_copy(tp_at(turn), tp_at(turn)).wait_recv())
-    shared_units = shared_all[...].reshape(tp_count * own_hidden, -1)
-    shared_sum = dot(shared_weight[...], shared_units).T[0:tokens]
-    routed = dot(spread[0], result_in[...]) + dot(spread[1], result_in[...])
-    moe_ref[...] = (routed + shared_sum).astype(moe_ref.dtype)
-
     def finish_ep(turn):
         pick_copy(ep_at(turn), me).wait_send()
-        result_copy(ep_at(turn), me).wait_send()
 
     loop(ep_count - 1, finish_ep)
 
@@ -827,6 +815,13 @@
                 side_copy(part, high_slot).wait_send()
 
     loop(up_hops + 1, finish_hop, 1)
+
+    loop(wide - 1, pass_row)
+    loop(tall - 1, pass_column)
+
+    loop(tp_count - 1, lambda turn: shared_copy(tp_at(turn), tp_at(turn)).wait_recv())
+    shared_units = shared_all[...].reshape(tp_count * own_hidden, -1)
+    shared_sum = dot(shared_weight[...], shared_units).T[0:tokens]
 
     def wait_far(turn):
         y = y_at(turn)
@@ -854,6 +849,11 @@
         mixed = dot(mix_weight[...], units)
         mixer_ref[span, :] = mixed.T.astype(mixer_ref.dtype)
 
+    loop(ep_count - 1, lambda turn: result_copy(ep_at(turn), ep_at(turn)).wait_recv())
+    own_result().wait()
+    routed = dot(spread[0], result_in[...]) + dot(spread[1], result_in[...])
+    moe_ref[...] = (routed + shared_sum).astype(moe_ref.dtype)
+
     def finish_row(turn):
         row_first(x_at(turn), x_me).wait_send()
         loop(tall, lambda y: column_part(y, x_at(turn)).wait_send())
@@ -862,6 +862,7 @@
         column_first(y_at(turn), y_me).wait_send()
         loop(wide, lambda x: row_part(x, y_at(turn)).wait_send())
 
+    loop(ep_count - 1, lambda turn: result_copy(ep_at(turn), me).wait_send())
     loop(wide - 1, finish_row)
     loop(tall - 1, finish_column)
 

time: 105 us -> 103 us (0.981)
  Pallas kernels: 102 us -> 99.2 us
    pallas_call x1, Pallas kernels: 102 us -> 99.2 us  [local(): pl.pallas_call(functools.partial(layer_kernel, cap, room), out_shape=[jax...]
where the time goes in v5:
time: 103 us; the launch traced here: 102 us
  Pallas kernels  99.2 us (96%)
  local copies, waits for them, and re-layouts  2.25 us (2%)
    pallas_call x1, Pallas kernels, local(): pl.pallas_call(functools.partial(layer_kernel, cap, room), out_shape=[jax...  99.2 us
    unnamed x4, local copies, waits for them, and re-layouts  2.25 us

profile of v5, /device:TPU:1, one launch (start us, length us, event | category | flops | bytes accessed | tf_op | source)
XLA Modules:
  0.0 102.2 jit_solution(15841295216072069436)
XLA Ops:
  0.6 99.2 %layer.1 = (bf16[768,128]{1,0:T(8,128)(2,1)}, bf16[192,128]{1,0:T(8,128)(2,1)}) custom-call(bf16[64,768]{1,0:T(8,128)(2,1)} %bitcast.15, bf16[64,768]{1,0:T(8,128)(2,1)} %bitcast.16, bf16[64,768]{1,0:T(8,128)(2,1)} %bitcast.17, f32[192,128]{1,0:T(8,128)} %bitcast.18, bf16[192,2048]{1,0:T(8,128)(2,1)} %input_ref.1, f32[1,2048]{1,0:T(1,128)} %bitcast.19, ...), custom_call_target="tpu_custom_call" | custom-call | flops 19327352832 | bytes 8388608 | tf_op jit(solution)/shard_map/layer/pallas_call | solution.py:921
  99.9 0.0 copy-start
  99.9 1.6 %copy.21 = bf16[768,128]{1,0:T(8,128)(2,1)} copy(bf16[768,128]{1,0:T(8,128)(2,1)} %get-tuple-element.4) | data formatting | bytes 393216
  101.5 0.0 copy-done
  101.5 0.6 copy.22
Async XLA Ops:
  99.9 1.6 %copy-start = (bf16[192,128]{1,0:T(8,128)(2,1)S(1)}, bf16[192,128]{1,0:T(8,128)(2,1)}, u32[]{:S(2)}) copy-start(bf16[192,128]{1,0:T(8,128)(2,1)} %get-tuple-element.5) | copy-start | bytes 147460
